TPU v7x, 512 devices: a whole 4x8x8 slice. The times are simulated.
512 devices in a mesh: ep: 128 (over z, y, core), tp: 4 (over x).
Axes of the slice: x: 4, y: 8, z: 8, core: 2. Of those that a mesh axis runs over, the one named last changes fastest.
Arguments:
- hidden_in: bfloat16 [2048, 1024], P('ep'), may hold values from -6 to 6
- prior_state: float32 [2048, 8, 128, 128], P('ep', 'tp'), may hold values from -4 to 4
- mix_gain: float32 [1024], replicated, may hold values from 0.1 to 1.9
- query_w: bfloat16 [1024, 1024], P(None, 'tp'), may hold values from -0.1875 to 0.1875
- key_w: bfloat16 [1024, 1024], P(None, 'tp'), may hold values from -0.1875 to 0.1875
- value_w: bfloat16 [1024, 1024], P(None, 'tp'), may hold values from -0.1875 to 0.1875
- decay_w: bfloat16 [1024, 8], P(None, 'tp'), may hold values from -0.1875 to 0.1875
- beta_w: bfloat16 [1024, 8], P(None, 'tp'), may hold values from -0.1875 to 0.1875
- decay_rate: float32 [8], P('tp'), may hold values from 0.05 to 3
- head_gain: float32 [128], replicated, may hold values from 0.1 to 1.9
- out_w: bfloat16 [1024, 1024], P('tp'), may hold values from -0.1875 to 0.1875
- ffn_gain: float32 [1024], replicated, may hold values from 0.1 to 1.9
- expert_ids: int32 [2048, 2], P('ep'), may hold values from 0 to 127, all different within a row; in each aligned block of 16 rows (0 to 15, 16 to 31, ...) at most 2 rows name the same one
- group_share: float32 [2048], P('ep'), may hold values from 0.3 to 1
- expert_share: float32 [2048, 2], P('ep'), may hold values from 0.1 to 1
- expert_gate: bfloat16 [128, 1024, 512], P('ep', None, 'tp'), may hold values from -0.1875 to 0.1875
- expert_up: bfloat16 [128, 1024, 512], P('ep', None, 'tp'), may hold values from -0.1875 to 0.1875
- expert_down: bfloat16 [128, 512, 1024], P('ep', 'tp'), may hold values from -0.25 to 0.25
- dense_gate: bfloat16 [4096, 1024], P('ep', 'tp'), may hold values from -0.1875 to 0.1875
- dense_up: bfloat16 [4096, 1024], P('ep', 'tp'), may hold values from -0.1875 to 0.1875
- dense_down: bfloat16 [4096, 1024], P('ep', 'tp'), may hold values from -0.25 to 0.25
- branch_gate: bfloat16 [1024], replicated, may hold values from -0.1875 to 0.1875
Outputs:
- layer_out: bfloat16 [2048, 1024], P('ep', 'tp')
Inputs may be any that keep to these rules, and one draw needn't show every extreme that they name: `expert_ids`: each row names 2 different experts. Among the rows of one device, no expert is named by more than 2 rows, and in every draw some expert is named by exactly 2 rows of some device.
All inputs are finite; a program needn't handle non-finite values.
Results may differ from a plain program's by a relative error of at most 0.02.
Values may be sent and summed in bfloat16 or wider, within the bound.
No kernel may reach another device: no remote copies, remote signals or barrier semaphores. Data moves between devices by JAX's collectives and lax.ppermute only.
A program may use at most 64 MiB of HBM per device.

v0:
```python
import functools

import jax
import jax.numpy as jnp
from jax import lax
from jax.experimental import pallas as pl
from jax.experimental.pallas import tpu as pltpu
from jax.sharding import Mesh
from jax.sharding import PartitionSpec as P

EP = ("z_hi", "z_lo", "y_hi", "y_lo", "c")
NEAR = ("z_lo", "y_lo", "c")
BF = jnp.bfloat16
F32 = jnp.float32


def rms_scale(values, gain, floor):
    return values * lax.rsqrt(jnp.mean(values * values, axis=-1, keepdims=True) + floor) * gain


def unit_rows(values):
    return values * lax.rsqrt(jnp.sum(values * values, axis=-1, keepdims=True) + 1.0)


def dot32(a, b):
    return jnp.dot(a, b, preferred_element_type=F32)


def slots_of(ids_ref, pick_ref, slot_ref, near, rows):
    choices = ids_ref.shape[0]
    row_ids = ids_ref[...].astype(F32)
    r_at = lax.broadcasted_iota(jnp.int32, (rows, rows), 0)
    c_at = lax.broadcasted_iota(jnp.int32, (rows, rows), 1)
    eye = jnp.where(r_at == c_at, 1.0, 0.0)
    col_ids = lax.dot_general(eye, row_ids, (((1,), (1,)), ((), ())), preferred_element_type=F32)
    row_slots, col_slots = [], []
    for j in range(choices):
        by_row = jnp.zeros((rows, rows), F32)
        by_col = jnp.zeros((rows, rows), F32)
        for o in range(choices):
            by_row += jnp.where(col_ids[:, o : o + 1] == row_ids[j : j + 1, :], 1.0, 0.0)
            by_col += jnp.where(col_ids[:, j : j + 1] == row_ids[o : o + 1, :], 1.0, 0.0)
        row_rank = jnp.sum(jnp.where(r_at < c_at, by_row, 0.0), axis=0, keepdims=True)
        col_rank = jnp.sum(jnp.where(c_at < r_at, by_col, 0.0), axis=1, keepdims=True)
        row_slots.append(row_ids[j : j + 1, :] * 2.0 + row_rank)
        col_slots.append(col_ids[:, j : j + 1] * 2.0 + col_rank)
    slot_ref[...] = jnp.concatenate(col_slots, axis=1).astype(jnp.int32)

    shape = (8, 2 * rows)
    at = lax.broadcasted_iota(jnp.int32, shape, 0)
    col = lax.broadcasted_iota(jnp.int32, shape, 1)
    slot = (at & 1).astype(F32)
    same_half = (at >= 4) == (col >= rows)
    for_expert = (at & 2) == 0
    token = jnp.where(col >= rows, col - rows, col).astype(F32)
    expert_keys = [
        jnp.where(
            same_half & for_expert, jnp.concatenate([found, found], axis=1) - slot, -1.0
        )
        for found in row_slots
    ]
    dense_key = jnp.where(same_half, jnp.where(for_expert, -1.0, token - slot), -1.0)
    dense_hit = [dense_key == 2.0 * n for n in range(near)]
    blocks = []
    for d in range(pick_ref.shape[0] // 8):
        hit = dense_hit[d // 16 % 2 * 4 + d // 2 % 2 * 2 + d % 2]
        for key in expert_keys:
            hit = hit | (key == 2.0 * d)
        blocks.append(jnp.where(hit, 1.0, 0.0))
    pick_ref[...] = jnp.concatenate(blocks, axis=0).astype(BF)


def mixer_body(
    near,
    hidden_ref,
    gain_ref,
    decay_ref,
    beta_ref,
    rate_ref,
    head_gain_ref,
    ids_ref,
    query_hbm,
    key_hbm,
    value_hbm,
    out_w_hbm,
    state_hbm,
    partial_ref,
    pick_ref,
    slot_ref,
    query_ref,
    key_ref,
    value_ref,
    out_w_ref,
    state_ref,
    sems,
):
    rows = hidden_ref.shape[0]
    heads = decay_ref.shape[0]
    dv = head_gain_ref.shape[1]
    dk = query_ref.shape[1] // heads
    groups = 4
    step = state_ref.shape[0] // groups

    def fetch(source, target, at):
        return pltpu.make_async_copy(source, target, sems.at[at])

    get_query = fetch(query_hbm, query_ref, 0)
    get_key = fetch(key_hbm, key_ref, 1)
    get_value = fetch(value_hbm, value_ref, 2)
    get_out = fetch(out_w_hbm, out_w_ref, 3)
    get_state = [
        fetch(
            state_hbm.at[pl.ds(g * step, step)], state_ref.at[pl.ds(g * step, step)], 4 + g
        )
        for g in range(groups)
    ]
    for copy in [get_query, get_key] + get_state + [get_value, get_out]:
        copy.start()
    slots_of(ids_ref, pick_ref, slot_ref, near, rows)
    wide = hidden_ref[...].astype(F32)
    normed = rms_scale(wide, gain_ref[...], 0.1).astype(BF)
    wide = normed.astype(F32)
    get_query.wait()
    q_all = dot32(normed, query_ref[...])
    get_key.wait()
    k_all = dot32(normed, key_ref[...])
    units = []
    for source in (q_all, k_all):
        for h in range(heads):
            units.append(unit_rows(source[:, h * dk : (h + 1) * dk]))
    stacked = jnp.concatenate(units, axis=0).astype(BF)
    pairs = heads * rows
    row_at = lax.broadcasted_iota(jnp.int32, stacked.shape, 0) % pairs
    zero = jnp.zeros_like(stacked)
    read = jnp.zeros((2 * pairs, dv), F32)
    for g in range(groups):
        get_state[g].wait()
        blocks = []
        for b in range(g * step // dk, (g + 1) * step // dk):
            blocks.append(jnp.where(row_at == (b % heads) * rows + b // heads, stacked, zero))
        state = state_ref[g * step : (g + 1) * step].astype(BF)
        read = read + dot32(jnp.concatenate(blocks, axis=1), state)
    get_value.wait()
    v_all = dot32(normed, value_ref[...])
    outs = []
    for h in range(heads):
        lanes = slice(h * dv, (h + 1) * dv)
        decay_in = jnp.sum(wide * decay_ref[h : h + 1, :].astype(F32), axis=1, keepdims=True)
        beta_in = jnp.sum(wide * beta_ref[h : h + 1, :].astype(F32), axis=1, keepdims=True)
        decay = jnp.exp(-rate_ref[h] * jax.nn.softplus(decay_in))
        meet = jnp.sum(units[h] * units[heads + h], axis=1, keepdims=True)
        meet = meet * jax.nn.sigmoid(beta_in)
        read_q = read[h * rows : (h + 1) * rows]
        read_k = read[pairs + h * rows : pairs + (h + 1) * rows]
        readout = decay * read_q + meet * (v_all[:, lanes] - decay * read_k)
        outs.append(rms_scale(readout, head_gain_ref[...], 0.01).astype(BF))
    head_out = jnp.concatenate(outs, axis=1)
    get_out.wait()
    partial = dot32(head_out, out_w_ref[...]).astype(BF)
    for t in range(partial_ref.shape[0]):
        partial_ref[t] = partial


def mixer(hidden, state, gain, query, key, value, decay, beta, rate, head_gain, out_w, ids, n_ep, n_tp, near):
    rows, width = hidden.shape
    vmem = pl.BlockSpec(memory_space=pltpu.VMEM)
    smem = pl.BlockSpec(memory_space=pltpu.SMEM)
    hbm = pl.BlockSpec(memory_space=pl.ANY)
    state = state.reshape(-1, state.shape[-1])
    return pl.pallas_call(
        functools.partial(mixer_body, near),
        out_shape=(
            jax.ShapeDtypeStruct((n_tp, rows, width), BF),
            jax.ShapeDtypeStruct((n_ep * 8, 2 * rows), BF),
            jax.ShapeDtypeStruct(ids.shape, jnp.int32),
        ),
        in_specs=[vmem] * 4 + [smem, vmem, vmem] + [hbm] * 5,
        out_specs=(vmem,) * 3,
        scratch_shapes=[
            pltpu.VMEM(query.shape, BF),
            pltpu.VMEM(key.shape, BF),
            pltpu.VMEM(value.shape, BF),
            pltpu.VMEM(out_w.shape, BF),
            pltpu.VMEM(state.shape, F32),
            pltpu.SemaphoreType.DMA((8,)),
        ],
        name="mixer",
    )(
        hidden,
        gain[None],
        decay.T,
        beta.T,
        rate,
        head_gain[None],
        ids.T,
        query,
        key,
        value,
        out_w,
        state,
    )


def spread_body(*refs):
    sources, target = refs[:-1], refs[-1]
    rows = sources[0].shape[0]
    for w, source in enumerate(sources):
        for c in range(target.shape[0]):
            target[c, w * rows : (w + 1) * rows, :] = source[...]


def spread(weights, count):
    rows, width = weights[0].shape
    vmem = pl.BlockSpec(memory_space=pltpu.VMEM)
    return pl.pallas_call(
        spread_body,
        out_shape=jax.ShapeDtypeStruct((count, len(weights) * rows, width), BF),
        in_specs=[vmem] * len(weights),
        out_specs=vmem,
        name="spread",
    )(*weights)


def exchange(blocks, axis):
    return lax.all_to_all(blocks, axis, split_axis=0, concat_axis=0, tiled=True)


def local(
    hidden_in,
    prior_state,
    mix_gain,
    query_w,
    key_w,
    value_w,
    decay_w,
    beta_w,
    decay_rate,
    head_gain,
    out_w,
    ffn_gain,
    expert_ids,
    group_share,
    expert_share,
    expert_gate,
    expert_up,
    expert_down,
    dense_gate,
    dense_up,
    dense_down,
    branch_gate,
):
    rows, width = hidden_in.shape
    n_ep = lax.axis_size(EP)
    n_tp = lax.axis_size("x")
    n_near = lax.axis_size(NEAR)
    quarter = width // n_tp
    cap = 2
    per_near = rows // n_near
    tp_at = lax.axis_index("x")
    hid = dense_gate.shape[0]

    copies = spread((dense_gate, dense_up, dense_down), n_near)
    dense_near = exchange(copies, NEAR).reshape(n_near, 3, hid, quarter)

    copies_out, pick, position = mixer(
        hidden_in,
        prior_state,
        mix_gain,
        query_w,
        key_w,
        value_w,
        decay_w,
        beta_w,
        decay_rate,
        head_gain,
        out_w,
        expert_ids,
        n_ep,
        n_tp,
        n_near,
    )
    partials = exchange(copies_out, "x")
    mix = jnp.sum(partials.astype(F32), axis=0)
    resid = (hidden_in.astype(F32) + mix).astype(BF)
    normed2 = rms_scale(resid.astype(F32), ffn_gain, 0.1).astype(BF)
    own = lax.dynamic_slice_in_dim(normed2, tp_at * quarter, quarter, 1)
    resid_own = lax.dynamic_slice_in_dim(resid, tp_at * quarter, quarter, 1).astype(F32)
    branch_weight = jax.nn.sigmoid(dot32(normed2, branch_gate))[:, None]

    block = cap + per_near
    halves = jnp.concatenate([own[:, : quarter // 2], own[:, quarter // 2 :]], axis=0)
    sent = dot32(pick, halves).astype(BF)
    n_hid = n_near * hid
    gate_near = dense_near[:, 0].reshape(n_hid, quarter)
    up_near = dense_near[:, 1].reshape(n_hid, quarter)
    down_near = dense_near[:, 2].reshape(n_hid, quarter)
    route_weight = (
        group_share[:, None] * expert_share / jnp.sum(expert_share, axis=1, keepdims=True)
    )
    fetch = (position[:, :, None] == jnp.arange(n_ep * cap)).astype(BF)
    ready = (sent, gate_near, up_near, down_near, fetch, route_weight, branch_weight, resid_own)
    ready = lax.optimization_barrier(ready)
    sent, gate_near, up_near, down_near, fetch, route_weight, branch_weight, resid_own = ready
    arrived = exchange(sent.reshape(n_ep, 8, quarter // 2), EP)
    arrived = arrived.reshape(n_ep, 2, block, quarter // 2)
    arrived = jnp.concatenate([arrived[:, 0], arrived[:, 1]], axis=2)
    moe_rows = arrived[:, :cap].reshape(n_ep * cap, quarter)
    dense_rows = arrived[:, cap:].reshape(n_ep * per_near, quarter)

    contract = (((1,), (1,)), ((), ()))
    gate_part = lax.dot_general(dense_rows, gate_near, contract, preferred_element_type=F32)
    up_part = lax.dot_general(dense_rows, up_near, contract, preferred_element_type=F32)
    share = n_hid // n_tp
    pre = jnp.stack(
        [gate_part.reshape(-1, n_tp, share), up_part.reshape(-1, n_tp, share)], axis=2
    ).astype(BF)
    pre = jnp.moveaxis(pre, 1, 0).reshape(n_tp, -1, 2 * share)
    moe_copies = jnp.broadcast_to(moe_rows, (n_tp, *moe_rows.shape))
    first = exchange(jnp.concatenate([moe_copies, pre], axis=2), "x")

    full_rows = jnp.moveaxis(first[:, :, :quarter], 0, 1).reshape(n_ep * cap, width)
    pre_sum = jnp.sum(first[:, :, quarter:].astype(F32), axis=0)
    dense_hidden = (jax.nn.silu(pre_sum[:, :share]) * pre_sum[:, share:]).astype(BF)
    gate_pre = dot32(full_rows, expert_gate[0])
    up_pre = dot32(full_rows, expert_up[0])
    hidden = (jax.nn.silu(gate_pre) * up_pre).astype(BF)
    expert_part = dot32(hidden, expert_down[0]).astype(BF)
    part_blocks = jnp.moveaxis(expert_part.reshape(n_ep * cap, n_tp, quarter), 1, 0)
    hidden_copies = jnp.broadcast_to(dense_hidden, (n_tp, *dense_hidden.shape))
    second = exchange(jnp.concatenate([part_blocks, hidden_copies], axis=2), "x")

    expert_out = jnp.sum(second[:, :, :quarter].astype(F32), axis=0).astype(BF)
    all_hidden = jnp.moveaxis(second[:, :, quarter:], 0, 1).reshape(n_ep * per_near, n_hid)
    dense_out = dot32(all_hidden, down_near).astype(BF)
    back = jnp.concatenate(
        [expert_out.reshape(n_ep, cap, quarter), dense_out.reshape(n_ep, per_near, quarter)], axis=1
    )
    returned = exchange(back, EP)

    slots = returned[:, :cap].reshape(n_ep * cap, quarter)
    per_choice = dot32(fetch.reshape(rows * 2, n_ep * cap), slots).reshape(rows, 2, quarter)
    moe = jnp.sum(per_choice * route_weight[:, :, None], axis=1)
    sides = [lax.axis_size(axis) for axis in EP]
    branch = jnp.sum(
        returned[:, cap:].astype(F32).reshape(*sides, per_near, quarter), axis=(0, 2)
    ).reshape(rows, quarter)
    return (resid_own + moe + branch_weight * branch).astype(BF)


def solution(mesh):
    torus = Mesh(mesh.devices.reshape(4, 2, 4, 2, 2, mesh.shape["tp"]), (*EP, "x"))
    placed = (
        P(EP, None),
        P(EP, "x", None, None),
        P(),
        P(None, "x"),
        P(None, "x"),
        P(None, "x"),
        P(None, "x"),
        P(None, "x"),
        P("x"),
        P(),
        P("x", None),
        P(),
        P(EP, None),
        P(EP),
        P(EP, None),
        P(EP, None, "x"),
        P(EP, None, "x"),
        P(EP, "x", None),
        P(EP, "x"),
        P(EP, "x"),
        P(EP, "x"),
        P(),
    )
    return jax.shard_map(local, mesh=torus, in_specs=placed, out_specs=P(EP, "x"), check_vma=False)
```

profile of v0, /device:TPU:1, one launch (start us, length us, event | category | flops | bytes accessed | tf_op | source)
XLA Modules:
  0.0 113.7 jit_solution(6965485298269370811)
XLA Ops:
  0.0 0.0 copy-start
  0.0 0.0 copy-start.7
  0.0 4.4 %mixer.1 = (bf16[4,16,1024]{2,1,0:T(8,128)(2,1)}, bf16[1024,32]{1,0:T(8,128)(2,1)}, s32[16,2]{1,0:T(8,128)}) custom-call(bf16[16,1024]{1,0:T(8,128)(2,1)} %hidden_ref.1, f32[1,1024]{1,0:T(1,128)} %bitcast.91, bf16[2,1024]{1,0:T(2,128)(2,1)} %bitcast.92, bf16[2,1024]{1,0:T(2,128)(2,1)} %bitcast.93, f32[2]{0:T(128)} %rate_ref.1, f32[1,128]{1,0:T(1,128)} %bitcast.95, ...), custom_call_target="tpu_custom_call" | custom-call | tf_op jit(solution)/shard_map/mixer/pallas_call | solution.py:170
  4.4 0.0 copy-start.4
  4.4 0.0 copy-start.5
  4.5 0.0 copy-start.2
  4.5 5.0 %all-to-all-start = ((bf16[4,16,1024]{2,1,0:T(8,128)(2,1)}), bf16[4,16,1024]{2,1,0:T(8,128)(2,1)S(1)}, u32[]{:S(2)}, u32[]{:S(2)}) async-start(bf16[4,16,1024]{2,1,0:T(8,128)(2,1)} %get-tuple-element.17), calls=%async_computation | async-start | bytes 262144 | tf_op jit(solution)/shard_map/all_to_all | solution.py:225
  9.4 0.8 copy.39
  10.2 0.1 fusion.25
  10.3 0.0 copy-done.8
  10.4 1.5 %spread.1 = bf16[8,96,256]{2,1,0:T(8,128)(2,1)} custom-call(bf16[32,256]{1,0:T(8,128)(2,1)} %refs_0_.1, bf16[32,256]{1,0:T(8,128)(2,1)} %refs_1_.1, bf16[32,256]{1,0:T(8,128)(2,1)} %refs_2_.1), custom_call_target="tpu_custom_call" | custom-call | tf_op jit(solution)/shard_map/spread/pallas_call | solution.py:215
  11.9 2.4 %all-to-all-done = bf16[4,16,1024]{2,1,0:T(8,128)(2,1)S(1)} async-done(((bf16[4,16,1024]{2,1,0:T(8,128)(2,1)}), bf16[4,16,1024]{2,1,0:T(8,128)(2,1)S(1)}, u32[]{:S(2)}, u32[]{:S(2)}) %all-to-all-start) | async-done | bytes 131104 | tf_op jit(solution)/shard_map/all_to_all | solution.py:225
  14.3 9.8 %all-to-all-start.1 = ((bf16[8,96,256]{2,1,0:T(8,128)(2,1)}), bf16[8,96,256]{2,1,0:T(8,128)(2,1)S(1)}, u32[]{:S(2)}, u32[]{:S(2)}) async-start(bf16[8,96,256]{2,1,0:T(8,128)(2,1)} %spread.1), calls=%async_computation.1 | async-start | bytes 786432 | tf_op jit(solution)/shard_map/all_to_all | solution.py:225
  24.1 0.1 fusion.20
  24.2 0.1 fusion.22
  24.4 0.1 fusion.8
  24.5 0.0 copy-done.2
  24.5 0.2 convolution_convert_fusion.1
  24.7 5.8 %all-to-all-done.1 = bf16[8,96,256]{2,1,0:T(8,128)(2,1)S(1)} async-done(((bf16[8,96,256]{2,1,0:T(8,128)(2,1)}), bf16[8,96,256]{2,1,0:T(8,128)(2,1)S(1)}, u32[]{:S(2)}, u32[]{:S(2)}) %all-to-all-start.1) | async-done | bytes 393248 | tf_op jit(solution)/shard_map/all_to_all | solution.py:225
  30.5 29.5 %all_to_all.30 = bf16[128,8,128]{2,1,0:T(8,128)(2,1)S(1)} all-to-all(bf16[128,8,128]{2,1,0:T(8,128)(2,1)S(1)} %bitcast.83), channel_id=1, replica_groups=mesh['z_hi'=4,'z_lo'=2,'y_hi'=4,'y_lo'=2,'c'=2,'x'=4] {'z_hi','z_lo','y_..., dimensions={0} | all-to-all | bytes 524288 | tf_op jit(solution)/shard_map/all_to_all | solution.py:225
  60.0 0.1 slice_bitcast_fusion.1
  60.1 0.2 fusion.14
  60.4 0.1 reshape.83
  60.4 0.1 copy.42
  60.6 0.1 reshape.101
  60.6 0.2 fusion.1
  60.8 0.2 fusion
  61.2 0.1 pad_maximum_fusion
  61.2 0.0 copy-start.1
  61.3 14.6 %all_to_all.31 = bf16[4,256,384]{1,2,0:T(8,128)(2,1)S(1)} all-to-all(bf16[4,256,384]{1,2,0:T(8,128)(2,1)S(1)} %pad_maximum_fusion), channel_id=1, replica_groups=mesh['z_hi'=4,'z_lo'=2,'y_hi'=4,'y_lo'=2,'c'=2,'x'=4] {'x'}, dimensions={0} | all-to-all | bytes 1572864 | tf_op jit(solution)/shard_map/all_to_all | solution.py:225
  75.9 0.0 copy-done.1
  75.9 0.3 fusion.12
  76.3 0.5 copy-done.3
  76.8 0.5 convolution_convert_fusion
  77.3 0.2 copy.46
  77.6 12.2 %all_to_all.32 = bf16[4,256,320]{1,2,0:T(8,128)(2,1)S(1)} all-to-all(bf16[4,256,320]{1,2,0:T(8,128)(2,1)S(1)} %pad_maximum_fusion.1), channel_id=1, replica_groups=mesh['z_hi'=4,'z_lo'=2,'y_hi'=4,'y_lo'=2,'c'=2,'x'=4] {'x'}, dimensions={0} | all-to-all | bytes 1310720 | tf_op jit(solution)/shard_map/all_to_all | solution.py:225
  89.7 0.1 slice_reduce_fusion
  89.8 0.1 copy.45
  89.9 0.1 reshape.90
  90.0 0.2 convolution_convert_fusion.2
  90.2 0.1 reshape.92
  90.3 0.3 pad_maximum_fusion.2
  90.6 21.9 %all_to_all.33 = bf16[128,4,256]{2,1,0:T(4,128)(2,1)S(1)} all-to-all(bf16[128,4,256]{2,1,0:T(4,128)(2,1)S(1)} %pad_maximum_fusion.2), channel_id=1, replica_groups=mesh['z_hi'=4,'z_lo'=2,'y_hi'=4,'y_lo'=2,'c'=2,'x'=4] {'z_hi','z_lo','y_..., dimensions={0} | all-to-all | bytes 524288 | tf_op jit(solution)/shard_map/all_to_all | solution.py:225
  112.5 0.2 fusion.32
  112.7 0.1 reshape.102
  112.8 0.1 convert_reduce_fusion.1
  112.9 0.1 fusion.3
  113.0 0.7 add_convert_fusion.1
  (26 shorter events, 0.4 us)
Async XLA Ops:
  0.0 76.3 %copy-start = (bf16[1,128,1024]{2,1,0:T(8,128)(2,1)S(1)}, bf16[1,128,1024]{2,1,0:T(8,128)(2,1)}, u32[]{:S(2)}) copy-start(bf16[1,128,1024]{2,1,0:T(8,128)(2,1)} %param.39) | copy-start | bytes 786436
  0.0 10.3 %copy-start.6 = (f32[16,2]{0,1:T(2,128)S(1)}, f32[16,2]{0,1:T(2,128)}, u32[]{:S(2)}) copy-start(f32[16,2]{0,1:T(2,128)} %param.36) | copy-start | bytes 388
  0.0 10.3 %copy-start.8 = (f32[16]{0:T(128)S(1)}, f32[16]{0:T(128)}, u32[]{:S(2)}) copy-start(f32[16]{0:T(128)} %param.35) | copy-start | bytes 196
  0.0 10.3 %copy-start.7 = (bf16[1024]{0:T(1024)(128)(2,1)S(1)}, bf16[1024]{0:T(1024)(128)(2,1)}, u32[]{:S(2)}) copy-start(bf16[1024]{0:T(1024)(128)(2,1)} %param.43) | copy-start | bytes 6148
  4.4 19.7 %copy-start.4 = (bf16[16,1024]{1,0:T(8,128)(2,1)S(1)}, bf16[16,1024]{1,0:T(8,128)(2,1)}, u32[]{:S(2)}) copy-start(bf16[16,1024]{1,0:T(8,128)(2,1)} %hidden_ref.1) | copy-start | bytes 98308
  4.4 19.8 %copy-start.5 = (f32[1024]{0:T(1024)S(1)}, f32[1024]{0:T(1024)}, u32[]{:S(2)}) copy-start(f32[1024]{0:T(1024)} %param.33) | copy-start | bytes 12292
  4.5 20.0 %copy-start.2 = (bf16[1024,32]{1,0:T(8,128)(2,1)S(1)}, bf16[1024,32]{1,0:T(8,128)(2,1)}, u32[]{:S(2)}) copy-start(bf16[1024,32]{1,0:T(8,128)(2,1)} %get-tuple-element.16) | copy-start | bytes 196612
  4.5 9.8 %all-to-all-start = ((bf16[4,16,1024]{2,1,0:T(8,128)(2,1)}), bf16[4,16,1024]{2,1,0:T(8,128)(2,1)S(1)}, u32[]{:S(2)}, u32[]{:S(2)}) async-start(bf16[4,16,1024]{2,1,0:T(8,128)(2,1)} %get-tuple-element.17), calls=%async_computation | async-start | bytes 262144 | tf_op jit(solution)/shard_map/all_to_all | solution.py:225
  14.3 16.2 %all-to-all-start.1 = ((bf16[8,96,256]{2,1,0:T(8,128)(2,1)}), bf16[8,96,256]{2,1,0:T(8,128)(2,1)S(1)}, u32[]{:S(2)}, u32[]{:S(2)}) async-start(bf16[8,96,256]{2,1,0:T(8,128)(2,1)} %spread.1), calls=%async_computation.1 | async-start | bytes 786432 | tf_op jit(solution)/shard_map/all_to_all | solution.py:225
  61.2 14.7 %copy-start.1 = (bf16[1,1024,128]{2,1,0:T(8,128)(2,1)S(1)}, bf16[1,1024,128]{2,1,0:T(8,128)(2,1)}, u32[]{:S(2)}) copy-start(bf16[1,1024,128]{2,1,0:T(8,128)(2,1)} %param.37) | copy-start | bytes 786436
  75.8 1.0 copy-start.3
where the time goes:
time: 114 us
  blocking collectives  78.2 us (69%)
  starting transfers between devices  14.8 us (13%)
  waiting for transfers between devices  8.18 us (7%)
  Pallas kernels  5.92 us (5%)
  local copies, waits for them, and re-layouts  2.41 us (2%)
  matrix products  1.99 us (2%)
  other arithmetic  1.96 us (2%)
    all_to_all x4, blocking collectives, exchange(): return lax.all_to_all(blocks, axis, split_axis=0, concat_axis=0, tiled=True)  78.2 us
    all_to_all x2, starting transfers between devices, exchange(): return lax.all_to_all(blocks, axis, split_axis=0, concat_axis=0, tiled=True)  14.8 us
    all_to_all x2, waiting for transfers between devices, exchange(): return lax.all_to_all(blocks, axis, split_axis=0, concat_axis=0, tiled=True)  8.18 us
    pallas_call x1, Pallas kernels, mixer(): pl.pallas_call(functools.partial(mixer_body, near), out_shape=(jax.ShapeD...  4.4 us
  transfers between devices with their start and end apart: 2, of which 2 were waited for; matrix products, arithmetic and copies ran while one was open for 1% of the time, Pallas kernels for 1%

commit v1 on v0

--- a/solution.py
+++ b/solution.py
@@ -26,7 +26,7 @@
     return jnp.dot(a, b, preferred_element_type=F32)
 
 
-def slots_of(ids_ref, pick_ref, slot_ref, near, rows):
+def slots_of(ids_ref, pick_ref, fetch_ref, near, rows):
     choices = ids_ref.shape[0]
     row_ids = ids_ref[...].astype(F32)
     r_at = lax.broadcasted_iota(jnp.int32, (rows, rows), 0)
@@ -44,7 +44,10 @@
         col_rank = jnp.sum(jnp.where(c_at < r_at, by_col, 0.0), axis=1, keepdims=True)
         row_slots.append(row_ids[j : j + 1, :] * 2.0 + row_rank)
         col_slots.append(col_ids[:, j : j + 1] * 2.0 + col_rank)
-    slot_ref[...] = jnp.concatenate(col_slots, axis=1).astype(jnp.int32)
+    place = lax.broadcasted_iota(jnp.int32, (rows, fetch_ref.shape[1]), 1).astype(F32)
+    fetch_ref[...] = jnp.concatenate(
+        [jnp.where(place == found, 1.0, 0.0) for found in col_slots], axis=0
+    ).astype(BF)
 
     shape = (8, 2 * rows)
     at = lax.broadcasted_iota(jnp.int32, shape, 0)
@@ -70,30 +73,25 @@
     pick_ref[...] = jnp.concatenate(blocks, axis=0).astype(BF)
 
 
-def mixer_body(
-    near,
-    hidden_ref,
-    gain_ref,
-    decay_ref,
-    beta_ref,
-    rate_ref,
-    head_gain_ref,
-    ids_ref,
-    query_hbm,
-    key_hbm,
-    value_hbm,
-    out_w_hbm,
-    state_hbm,
-    partial_ref,
-    pick_ref,
-    slot_ref,
-    query_ref,
-    key_ref,
-    value_ref,
-    out_w_ref,
-    state_ref,
-    sems,
-):
+def mixer_body(near, *refs):
+    rate_ref, sources, targets, buffers = refs[0], refs[1:12], refs[12:15], refs[15:29]
+    sems = refs[29]
+    (
+        hidden_ref,
+        gain_ref,
+        decay_ref,
+        beta_ref,
+        head_gain_ref,
+        ids_ref,
+        query_ref,
+        key_ref,
+        value_ref,
+        out_w_ref,
+        state_ref,
+        partial_ref,
+        pick_ref,
+        fetch_ref,
+    ) = buffers
     rows = hidden_ref.shape[0]
     heads = decay_ref.shape[0]
     dv = head_gain_ref.shape[1]
@@ -101,28 +99,31 @@
     groups = 4
     step = state_ref.shape[0] // groups
 
-    def fetch(source, target, at):
+    def copy_of(source, target, at):
         return pltpu.make_async_copy(source, target, sems.at[at])
 
-    get_query = fetch(query_hbm, query_ref, 0)
-    get_key = fetch(key_hbm, key_ref, 1)
-    get_value = fetch(value_hbm, value_ref, 2)
-    get_out = fetch(out_w_hbm, out_w_ref, 3)
+    gets = [copy_of(sources[n], buffers[n], n) for n in range(10)]
     get_state = [
-        fetch(
-            state_hbm.at[pl.ds(g * step, step)], state_ref.at[pl.ds(g * step, step)], 4 + g
+        copy_of(
+            sources[10].at[pl.ds(g * step, step)], state_ref.at[pl.ds(g * step, step)], 10 + g
         )
         for g in range(groups)
     ]
-    for copy in [get_query, get_key] + get_state + [get_value, get_out]:
+    puts = [copy_of(buffers[11 + n], targets[n], 14 + n) for n in range(3)]
+    for copy in gets[:8] + get_state + gets[8:]:
         copy.start()
-    slots_of(ids_ref, pick_ref, slot_ref, near, rows)
+    gets[5].wait()
+    slots_of(ids_ref, pick_ref, fetch_ref, near, rows)
+    puts[1].start()
+    puts[2].start()
+    for copy in gets[:5]:
+        copy.wait()
     wide = hidden_ref[...].astype(F32)
     normed = rms_scale(wide, gain_ref[...], 0.1).astype(BF)
     wide = normed.astype(F32)
-    get_query.wait()
+    gets[6].wait()
     q_all = dot32(normed, query_ref[...])
-    get_key.wait()
+    gets[7].wait()
     k_all = dot32(normed, key_ref[...])
     units = []
     for source in (q_all, k_all):
@@ -140,7 +141,7 @@
             blocks.append(jnp.where(row_at == (b % heads) * rows + b // heads, stacked, zero))
         state = state_ref[g * step : (g + 1) * step].astype(BF)
         read = read + dot32(jnp.concatenate(blocks, axis=1), state)
-    get_value.wait()
+    gets[8].wait()
     v_all = dot32(normed, value_ref[...])
     outs = []
     for h in range(heads):
@@ -155,50 +156,46 @@
         readout = decay * read_q + meet * (v_all[:, lanes] - decay * read_k)
         outs.append(rms_scale(readout, head_gain_ref[...], 0.01).astype(BF))
     head_out = jnp.concatenate(outs, axis=1)
-    get_out.wait()
+    gets[9].wait()
     partial = dot32(head_out, out_w_ref[...]).astype(BF)
     for t in range(partial_ref.shape[0]):
         partial_ref[t] = partial
+    puts[0].start()
+    for copy in puts:
+        copy.wait()
 
 
 def mixer(hidden, state, gain, query, key, value, decay, beta, rate, head_gain, out_w, ids, n_ep, n_tp, near):
     rows, width = hidden.shape
-    vmem = pl.BlockSpec(memory_space=pltpu.VMEM)
     smem = pl.BlockSpec(memory_space=pltpu.SMEM)
-    hbm = pl.BlockSpec(memory_space=pl.ANY)
-    state = state.reshape(-1, state.shape[-1])
-    return pl.pallas_call(
-        functools.partial(mixer_body, near),
-        out_shape=(
-            jax.ShapeDtypeStruct((n_tp, rows, width), BF),
-            jax.ShapeDtypeStruct((n_ep * 8, 2 * rows), BF),
-            jax.ShapeDtypeStruct(ids.shape, jnp.int32),
-        ),
-        in_specs=[vmem] * 4 + [smem, vmem, vmem] + [hbm] * 5,
-        out_specs=(vmem,) * 3,
-        scratch_shapes=[
-            pltpu.VMEM(query.shape, BF),
-            pltpu.VMEM(key.shape, BF),
-            pltpu.VMEM(value.shape, BF),
-            pltpu.VMEM(out_w.shape, BF),
-            pltpu.VMEM(state.shape, F32),
-            pltpu.SemaphoreType.DMA((8,)),
-        ],
-        name="mixer",
-    )(
+    anywhere = pl.BlockSpec(memory_space=pl.ANY)
+    arrays = (
         hidden,
         gain[None],
         decay.T,
         beta.T,
-        rate,
         head_gain[None],
         ids.T,
         query,
         key,
         value,
         out_w,
-        state,
-    )
+        state.reshape(-1, state.shape[-1]),
+    )
+    outs = (
+        jax.ShapeDtypeStruct((n_tp, rows, width), BF),
+        jax.ShapeDtypeStruct((n_ep * 8, 2 * rows), BF),
+        jax.ShapeDtypeStruct((ids.size, 2 * n_ep), BF),
+    )
+    return pl.pallas_call(
+        functools.partial(mixer_body, near),
+        out_shape=outs,
+        in_specs=[smem] + [anywhere] * len(arrays),
+        out_specs=(anywhere,) * len(outs),
+        scratch_shapes=[pltpu.VMEM(a.shape, a.dtype) for a in (*arrays, *outs)]
+        + [pltpu.SemaphoreType.DMA((17,))],
+        name="mixer",
+    )(rate, *arrays)
 
 
 def spread_body(*refs):
@@ -262,7 +259,7 @@
     copies = spread((dense_gate, dense_up, dense_down), n_near)
     dense_near = exchange(copies, NEAR).reshape(n_near, 3, hid, quarter)
 
-    copies_out, pick, position = mixer(
+    copies_out, pick, fetch = mixer(
         hidden_in,
         prior_state,
         mix_gain,
@@ -285,7 +282,9 @@
     normed2 = rms_scale(resid.astype(F32), ffn_gain, 0.1).astype(BF)
     own = lax.dynamic_slice_in_dim(normed2, tp_at * quarter, quarter, 1)
     resid_own = lax.dynamic_slice_in_dim(resid, tp_at * quarter, quarter, 1).astype(F32)
-    branch_weight = jax.nn.sigmoid(dot32(normed2, branch_gate))[:, None]
+    gate_wide = branch_gate.astype(F32)
+    branch_dot = jnp.sum(normed2.astype(F32) * gate_wide, axis=1, keepdims=True)
+    branch_weight = jax.nn.sigmoid(branch_dot)
 
     block = cap + per_near
     halves = jnp.concatenate([own[:, : quarter // 2], own[:, quarter // 2 :]], axis=0)
@@ -297,10 +296,13 @@
     route_weight = (
         group_share[:, None] * expert_share / jnp.sum(expert_share, axis=1, keepdims=True)
     )
-    fetch = (position[:, :, None] == jnp.arange(n_ep * cap)).astype(BF)
-    ready = (sent, gate_near, up_near, down_near, fetch, route_weight, branch_weight, resid_own)
-    ready = lax.optimization_barrier(ready)
-    sent, gate_near, up_near, down_near, fetch, route_weight, branch_weight, resid_own = ready
+    first_weight, second_weight = route_weight[:, :1], route_weight[:, 1:]
+    sent, gate_near, up_near, down_near, fetch = lax.optimization_barrier(
+        (sent, gate_near, up_near, down_near, fetch)
+    )
+    sent, first_weight, second_weight, branch_weight, resid_own = lax.optimization_barrier(
+        (sent, first_weight, second_weight, branch_weight, resid_own)
+    )
     arrived = exchange(sent.reshape(n_ep, 8, quarter // 2), EP)
     arrived = arrived.reshape(n_ep, 2, block, quarter // 2)
     arrived = jnp.concatenate([arrived[:, 0], arrived[:, 1]], axis=2)
@@ -338,8 +340,8 @@
     returned = exchange(back, EP)
 
     slots = returned[:, :cap].reshape(n_ep * cap, quarter)
-    per_choice = dot32(fetch.reshape(rows * 2, n_ep * cap), slots).reshape(rows, 2, quarter)
-    moe = jnp.sum(per_choice * route_weight[:, :, None], axis=1)
+    per_choice = dot32(fetch, slots)
+    moe = per_choice[:rows] * first_weight + per_choice[rows:] * second_weight
     sides = [lax.axis_size(axis) for axis in EP]
     branch = jnp.sum(
         returned[:, cap:].astype(F32).reshape(*sides, per_near, quarter), axis=(0, 2)

time: 114 us -> 115 us (level)
  no operation moved by 1% of the time
where the time goes in v1:
time: 115 us; the launch traced here: 114 us
  blocking collectives  78.2 us (68%)
  starting transfers between devices  14.8 us (13%)
  waiting for transfers between devices  9 us (8%)
  Pallas kernels  6.34 us (6%)
  other arithmetic  1.97 us (2%)
  matrix products  1.89 us (2%)
  local copies, waits for them, and re-layouts  1.64 us (1%)
    all_to_all x4, blocking collectives, exchange(): return lax.all_to_all(blocks, axis, split_axis=0, concat_axis=0, tiled=True)  78.2 us
    all_to_all x2, starting transfers between devices, exchange(): return lax.all_to_all(blocks, axis, split_axis=0, concat_axis=0, tiled=True)  14.8 us
    all_to_all x2, waiting for transfers between devices, exchange(): return lax.all_to_all(blocks, axis, split_axis=0, concat_axis=0, tiled=True)  9 us
    pallas_call x1, Pallas kernels, mixer(): pl.pallas_call(functools.partial(mixer_body, near), out_shape=outs, in_sp...  4.81 us
  transfers between devices with their start and end apart: 2, of which 2 were waited for; matrix products, arithmetic and copies ran while one was open for 1% of the time, Pallas kernels for 1%

profile of v1, /device:TPU:1, one launch (start us, length us, event | category | flops | bytes accessed | tf_op | source)
XLA Modules:
  0.0 114.2 jit_solution(10527226634960099340)
XLA Ops:
  0.0 0.0 copy-start
  0.0 0.0 copy-start.8
  0.0 4.8 %mixer.1 = (bf16[4,16,1024]{2,1,0:T(8,128)(2,1)}, bf16[1024,32]{1,0:T(8,128)(2,1)}, bf16[32,256]{1,0:T(8,128)(2,1)}) custom-call(f32[2]{0:T(128)} %refs_0_.2, bf16[16,1024]{1,0:T(8,128)(2,1)} %refs_1_.2, f32[1,1024]{1,0:T(1,128)} %bitcast.79, bf16[2,1024]{1,0:T(2,128)(2,1)} %bitcast.80, bf16[2,1024]{1,0:T(2,128)(2,1)} %bitcast.81, f32[1,128]{1,0:T(1,128)} %bitcast.85, ...), custom_call_target="tpu_custom_call" | custom-call | tf_op jit(solution)/shard_map/mixer/pallas_call | solution.py:190
  4.8 0.0 copy-start.4
  4.8 0.0 copy-start.6
  4.9 0.0 copy-start.2
  4.9 5.0 %all-to-all-start = ((bf16[4,16,1024]{2,1,0:T(8,128)(2,1)}), bf16[4,16,1024]{2,1,0:T(8,128)(2,1)S(1)}, u32[]{:S(2)}, u32[]{:S(2)}) async-start(bf16[4,16,1024]{2,1,0:T(8,128)(2,1)} %get-tuple-element.19), calls=%async_computation | async-start | bytes 262144 | tf_op jit(solution)/shard_map/all_to_all | solution.py:222
  9.8 0.0 copy-done.7
  9.9 0.0 copy-done.9
  9.9 0.0 copy-done.8
  9.9 1.5 %spread.1 = bf16[8,96,256]{2,1,0:T(8,128)(2,1)} custom-call(bf16[32,256]{1,0:T(8,128)(2,1)} %refs_0_.3, bf16[32,256]{1,0:T(8,128)(2,1)} %refs_1_.3, bf16[32,256]{1,0:T(8,128)(2,1)} %refs_2_.1), custom_call_target="tpu_custom_call" | custom-call | tf_op jit(solution)/shard_map/spread/pallas_call | solution.py:212
  11.5 3.2 %all-to-all-done = bf16[4,16,1024]{2,1,0:T(8,128)(2,1)S(1)} async-done(((bf16[4,16,1024]{2,1,0:T(8,128)(2,1)}), bf16[4,16,1024]{2,1,0:T(8,128)(2,1)S(1)}, u32[]{:S(2)}, u32[]{:S(2)}) %all-to-all-start) | async-done | bytes 131104 | tf_op jit(solution)/shard_map/all_to_all | solution.py:222
  14.7 9.8 %all-to-all-start.1 = ((bf16[8,96,256]{2,1,0:T(8,128)(2,1)}), bf16[8,96,256]{2,1,0:T(8,128)(2,1)S(1)}, u32[]{:S(2)}, u32[]{:S(2)}) async-start(bf16[8,96,256]{2,1,0:T(8,128)(2,1)} %spread.1), calls=%async_computation.1 | async-start | bytes 786432 | tf_op jit(solution)/shard_map/all_to_all | solution.py:222
  24.5 0.0 copy-done.4
  24.5 0.1 fusion.14
  24.6 0.0 copy-done.6
  24.6 0.2 multiply_reduce_fusion
  24.9 0.2 convolution_convert_fusion.1
  25.1 5.8 %all-to-all-done.1 = bf16[8,96,256]{2,1,0:T(8,128)(2,1)S(1)} async-done(((bf16[8,96,256]{2,1,0:T(8,128)(2,1)}), bf16[8,96,256]{2,1,0:T(8,128)(2,1)S(1)}, u32[]{:S(2)}, u32[]{:S(2)}) %all-to-all-start.1) | async-done | bytes 393248 | tf_op jit(solution)/shard_map/all_to_all | solution.py:222
  30.9 29.5 %all_to_all.30 = bf16[128,8,128]{2,1,0:T(8,128)(2,1)S(1)} all-to-all(bf16[128,8,128]{2,1,0:T(8,128)(2,1)S(1)} %bitcast.71), channel_id=1, replica_groups=mesh['z_hi'=4,'z_lo'=2,'y_hi'=4,'y_lo'=2,'c'=2,'x'=4] {'z_hi','z_lo','y_..., dimensions={0} | all-to-all | bytes 524288 | tf_op jit(solution)/shard_map/all_to_all | solution.py:222
  60.4 0.1 slice_bitcast_fusion.1
  60.5 0.2 fusion.8
  60.8 0.1 reshape.104
  60.8 0.1 copy.38
  61.0 0.1 reshape.120
  61.0 0.2 fusion.1
  61.2 0.2 fusion
  61.6 0.1 pad_maximum_fusion
  61.6 0.0 copy-start.1
  61.6 14.5 %all_to_all.31 = bf16[4,256,384]{1,2,0:T(8,128)(2,1)S(1)} all-to-all(bf16[4,256,384]{1,2,0:T(8,128)(2,1)S(1)} %pad_maximum_fusion), channel_id=1, replica_groups=mesh['z_hi'=4,'z_lo'=2,'y_hi'=4,'y_lo'=2,'c'=2,'x'=4] {'x'}, dimensions={0} | all-to-all | bytes 1572864 | tf_op jit(solution)/shard_map/all_to_all | solution.py:222
  76.3 0.3 fusion.6
  76.7 0.0 copy-done
  76.7 0.5 copy-done.3
  77.1 0.6 convolution_convert_fusion
  77.7 0.2 copy.42
  78.0 12.1 %all_to_all.32 = bf16[4,256,320]{1,2,0:T(8,128)(2,1)S(1)} all-to-all(bf16[4,256,320]{1,2,0:T(8,128)(2,1)S(1)} %pad_maximum_fusion.1), channel_id=1, replica_groups=mesh['z_hi'=4,'z_lo'=2,'y_hi'=4,'y_lo'=2,'c'=2,'x'=4] {'x'}, dimensions={0} | all-to-all | bytes 1310720 | tf_op jit(solution)/shard_map/all_to_all | solution.py:222
  90.1 0.1 slice_reduce_fusion
  90.2 0.1 copy.41
  90.3 0.1 reshape.111
  90.4 0.2 convolution_convert_fusion.2
  90.6 0.1 reshape.113
  90.7 0.3 pad_maximum_fusion.2
  91.0 22.0 %all_to_all.33 = bf16[128,4,256]{2,1,0:T(4,128)(2,1)S(1)} all-to-all(bf16[128,4,256]{2,1,0:T(4,128)(2,1)S(1)} %pad_maximum_fusion.2), channel_id=1, replica_groups=mesh['z_hi'=4,'z_lo'=2,'y_hi'=4,'y_lo'=2,'c'=2,'x'=4] {'z_hi','z_lo','y_..., dimensions={0} | all-to-all | bytes 524288 | tf_op jit(solution)/shard_map/all_to_all | solution.py:222
  112.9 0.2 fusion.30
  113.1 0.1 convert_reduce_fusion.1
  113.3 0.1 reshape.114
  113.3 0.1 fusion.32
  113.5 0.7 fusion.22
  (27 shorter events, 0.4 us)
Async XLA Ops:
  0.0 76.7 %copy-start = (bf16[1,128,1024]{2,1,0:T(8,128)(2,1)S(1)}, bf16[1,128,1024]{2,1,0:T(8,128)(2,1)}, u32[]{:S(2)}) copy-start(bf16[1,128,1024]{2,1,0:T(8,128)(2,1)} %param.39) | copy-start | bytes 786436
  0.0 9.8 %copy-start.7 = (f32[16,2]{0,1:T(2,128)S(1)}, f32[16,2]{0,1:T(2,128)}, u32[]{:S(2)}) copy-start(f32[16,2]{0,1:T(2,128)} %param.36) | copy-start | bytes 388
  0.0 9.9 %copy-start.9 = (f32[16]{0:T(128)S(1)}, f32[16]{0:T(128)}, u32[]{:S(2)}) copy-start(f32[16]{0:T(128)} %param.35) | copy-start | bytes 196
  0.0 9.9 %copy-start.8 = (bf16[1024]{0:T(1024)(128)(2,1)S(1)}, bf16[1024]{0:T(1024)(128)(2,1)}, u32[]{:S(2)}) copy-start(bf16[1024]{0:T(1024)(128)(2,1)} %param.43) | copy-start | bytes 6148
  4.8 19.7 %copy-start.4 = (bf16[16,1024]{1,0:T(8,128)(2,1)S(1)}, bf16[16,1024]{1,0:T(8,128)(2,1)}, u32[]{:S(2)}) copy-start(bf16[16,1024]{1,0:T(8,128)(2,1)} %refs_1_.2) | copy-start | bytes 98308
  4.8 19.8 %copy-start.6 = (f32[1024]{0:T(1024)S(1)}, f32[1024]{0:T(1024)}, u32[]{:S(2)}) copy-start(f32[1024]{0:T(1024)} %param.33) | copy-start | bytes 12292
  4.9 20.0 %copy-start.2 = (bf16[1024,32]{1,0:T(8,128)(2,1)S(1)}, bf16[1024,32]{1,0:T(8,128)(2,1)}, u32[]{:S(2)}) copy-start(bf16[1024,32]{1,0:T(8,128)(2,1)} %get-tuple-element.18) | copy-start | bytes 196612
  4.9 9.8 %all-to-all-start = ((bf16[4,16,1024]{2,1,0:T(8,128)(2,1)}), bf16[4,16,1024]{2,1,0:T(8,128)(2,1)S(1)}, u32[]{:S(2)}, u32[]{:S(2)}) async-start(bf16[4,16,1024]{2,1,0:T(8,128)(2,1)} %get-tuple-element.19), calls=%async_computation | async-start | bytes 262144 | tf_op jit(solution)/shard_map/all_to_all | solution.py:222
  14.7 16.2 %all-to-all-start.1 = ((bf16[8,96,256]{2,1,0:T(8,128)(2,1)}), bf16[8,96,256]{2,1,0:T(8,128)(2,1)S(1)}, u32[]{:S(2)}, u32[]{:S(2)}) async-start(bf16[8,96,256]{2,1,0:T(8,128)(2,1)} %spread.1), calls=%async_computation.1 | async-start | bytes 786432 | tf_op jit(solution)/shard_map/all_to_all | solution.py:222
  61.6 14.7 %copy-start.1 = (bf16[1,1024,128]{2,1,0:T(8,128)(2,1)S(1)}, bf16[1,1024,128]{2,1,0:T(8,128)(2,1)}, u32[]{:S(2)}) copy-start(bf16[1,1024,128]{2,1,0:T(8,128)(2,1)} %param.37) | copy-start | bytes 786436
  76.2 1.0 copy-start.3
  90.3 23.0 %copy-start.5 = (bf16[32,256]{1,0:T(8,128)(2,1)S(1)}, bf16[32,256]{1,0:T(8,128)(2,1)}, u32[]{:S(2)}) copy-start(bf16[32,256]{1,0:T(8,128)(2,1)} %get-tuple-element.23) | copy-start | bytes 49156

commit v2 on v1

--- a/solution.py
+++ b/solution.py
@@ -290,15 +290,17 @@
     halves = jnp.concatenate([own[:, : quarter // 2], own[:, quarter // 2 :]], axis=0)
     sent = dot32(pick, halves).astype(BF)
     n_hid = n_near * hid
-    gate_near = dense_near[:, 0].reshape(n_hid, quarter)
-    up_near = dense_near[:, 1].reshape(n_hid, quarter)
+    share = n_hid // n_tp
+    pairs_near = dense_near[:, :2].reshape(n_tp, -1, 2, hid, quarter)
+    both_near = jnp.swapaxes(pairs_near, 1, 2).reshape(2 * n_hid, quarter)
     down_near = dense_near[:, 2].reshape(n_hid, quarter)
+    expert_both = jnp.concatenate([expert_gate[0], expert_up[0]], axis=1)
     route_weight = (
         group_share[:, None] * expert_share / jnp.sum(expert_share, axis=1, keepdims=True)
     )
     first_weight, second_weight = route_weight[:, :1], route_weight[:, 1:]
-    sent, gate_near, up_near, down_near, fetch = lax.optimization_barrier(
-        (sent, gate_near, up_near, down_near, fetch)
+    sent, both_near, down_near, fetch, expert_both = lax.optimization_barrier(
+        (sent, both_near, down_near, fetch, expert_both)
     )
     sent, first_weight, second_weight, branch_weight, resid_own = lax.optimization_barrier(
         (sent, first_weight, second_weight, branch_weight, resid_own)
@@ -310,30 +312,30 @@
     dense_rows = arrived[:, cap:].reshape(n_ep * per_near, quarter)
 
     contract = (((1,), (1,)), ((), ()))
-    gate_part = lax.dot_general(dense_rows, gate_near, contract, preferred_element_type=F32)
-    up_part = lax.dot_general(dense_rows, up_near, contract, preferred_element_type=F32)
-    share = n_hid // n_tp
-    pre = jnp.stack(
-        [gate_part.reshape(-1, n_tp, share), up_part.reshape(-1, n_tp, share)], axis=2
+    pre = lax.dot_general(both_near, dense_rows, contract, preferred_element_type=F32)
+    pre = pre.astype(BF).reshape(n_tp, 2 * share, -1)
+    moe_copies = jnp.broadcast_to(moe_rows, (n_tp, *moe_rows.shape))
+    first = exchange(jnp.concatenate([moe_copies, pre], axis=1), "x")
+
+    n_rows = n_ep * cap
+    pre_sum = jnp.sum(first[:, n_rows:].astype(F32), axis=0)
+    dense_hidden = (jax.nn.silu(pre_sum[:share]) * pre_sum[share:]).astype(BF)
+    full_rows = jnp.concatenate([first[t, :n_rows] for t in range(n_tp)], axis=1)
+    both_pre = dot32(full_rows, expert_both)
+    wide = both_pre.shape[1] // 2
+    hidden = (jax.nn.silu(both_pre[:, :wide]) * both_pre[:, wide:]).astype(BF)
+    expert_part = dot32(hidden, expert_down[0]).astype(BF)
+    part_blocks = jnp.stack(
+        [expert_part[:, t * quarter : (t + 1) * quarter] for t in range(n_tp)], axis=0
+    )
+    hidden_copies = jnp.broadcast_to(dense_hidden, (n_tp, *dense_hidden.shape))
+    second = exchange(jnp.concatenate([part_blocks, hidden_copies], axis=1), "x")
+
+    expert_out = jnp.sum(second[:, :n_rows].astype(F32), axis=0).astype(BF)
+    all_hidden = second[:, n_rows:].reshape(n_hid, -1)
+    dense_out = lax.dot_general(
+        all_hidden, down_near, (((0,), (0,)), ((), ())), preferred_element_type=F32
     ).astype(BF)
-    pre = jnp.moveaxis(pre, 1, 0).reshape(n_tp, -1, 2 * share)
-    moe_copies = jnp.broadcast_to(moe_rows, (n_tp, *moe_rows.shape))
-    first = exchange(jnp.concatenate([moe_copies, pre], axis=2), "x")
-
-    full_rows = jnp.moveaxis(first[:, :, :quarter], 0, 1).reshape(n_ep * cap, width)
-    pre_sum = jnp.sum(first[:, :, quarter:].astype(F32), axis=0)
-    dense_hidden = (jax.nn.silu(pre_sum[:, :share]) * pre_sum[:, share:]).astype(BF)
-    gate_pre = dot32(full_rows, expert_gate[0])
-    up_pre = dot32(full_rows, expert_up[0])
-    hidden = (jax.nn.silu(gate_pre) * up_pre).astype(BF)
-    expert_part = dot32(hidden, expert_down[0]).astype(BF)
-    part_blocks = jnp.moveaxis(expert_part.reshape(n_ep * cap, n_tp, quarter), 1, 0)
-    hidden_copies = jnp.broadcast_to(dense_hidden, (n_tp, *dense_hidden.shape))
-    second = exchange(jnp.concatenate([part_blocks, hidden_copies], axis=2), "x")
-
-    expert_out = jnp.sum(second[:, :, :quarter].astype(F32), axis=0).astype(BF)
-    all_hidden = jnp.moveaxis(second[:, :, quarter:], 0, 1).reshape(n_ep * per_near, n_hid)
-    dense_out = dot32(all_hidden, down_near).astype(BF)
     back = jnp.concatenate(
         [expert_out.reshape(n_ep, cap, quarter), dense_out.reshape(n_ep, per_near, quarter)], axis=1
     )

time: 115 us -> 113 us (0.983)
  no operation moved by 1% of the time
where the time goes in v2:
time: 113 us
  blocking collectives  78.1 us (69%)
  starting transfers between devices  14.6 us (13%)
  waiting for transfers between devices  8.87 us (8%)
  Pallas kernels  6.38 us (6%)
  other arithmetic  2 us (2%)
  matrix products  1.42 us (1%)
    all_to_all x4, blocking collectives, exchange(): return lax.all_to_all(blocks, axis, split_axis=0, concat_axis=0, tiled=True)  78.1 us
    all_to_all x2, starting transfers between devices, exchange(): return lax.all_to_all(blocks, axis, split_axis=0, concat_axis=0, tiled=True)  14.6 us
    all_to_all x2, waiting for transfers between devices, exchange(): return lax.all_to_all(blocks, axis, split_axis=0, concat_axis=0, tiled=True)  8.87 us
    pallas_call x1, Pallas kernels, mixer(): pl.pallas_call(functools.partial(mixer_body, near), out_shape=outs, in_sp...  4.81 us
  transfers between devices with their start and end apart: 2, of which 2 were waited for; matrix products, arithmetic and copies ran while one was open for 1% of the time, Pallas kernels for 1%

profile of v2, /device:TPU:1, one launch (start us, length us, event | category | flops | bytes accessed | tf_op | source)
XLA Modules:
  0.0 112.5 jit_solution(111554691475983179)
XLA Ops:
  0.0 0.0 copy-start
  0.0 0.0 copy-start.8
  0.0 0.0 copy-start.2
  0.0 0.0 copy-start.3
  0.0 4.8 %mixer.1 = (bf16[4,16,1024]{2,1,0:T(8,128)(2,1)}, bf16[1024,32]{1,0:T(8,128)(2,1)}, bf16[32,256]{1,0:T(8,128)(2,1)}) custom-call(f32[2]{0:T(128)} %refs_0_.2, bf16[16,1024]{1,0:T(8,128)(2,1)} %refs_1_.2, f32[1,1024]{1,0:T(1,128)} %bitcast.71, bf16[2,1024]{1,0:T(2,128)(2,1)} %bitcast.72, bf16[2,1024]{1,0:T(2,128)(2,1)} %bitcast.73, f32[1,128]{1,0:T(1,128)} %bitcast.77, ...), custom_call_target="tpu_custom_call" | custom-call | tf_op jit(solution)/shard_map/mixer/pallas_call | solution.py:190
  4.9 4.8 %all-to-all-start = ((bf16[4,16,1024]{2,1,0:T(8,128)(2,1)}), bf16[4,16,1024]{2,1,0:T(8,128)(2,1)S(1)}, u32[]{:S(2)}, u32[]{:S(2)}) async-start(bf16[4,16,1024]{2,1,0:T(8,128)(2,1)} %get-tuple-element.19), calls=%async_computation | async-start | bytes 262144 | tf_op jit(solution)/shard_map/all_to_all | solution.py:222
  9.7 0.0 copy-done.7
  9.7 0.0 copy-done.9
  9.8 0.0 copy-done.8
  9.8 0.0 copy-start.6
  9.8 0.0 copy-start.1
  9.8 1.6 %spread.1 = bf16[8,96,256]{2,1,0:T(8,128)(2,1)} custom-call(bf16[32,256]{1,0:T(8,128)(2,1)} %refs_0_.3, bf16[32,256]{1,0:T(8,128)(2,1)} %refs_1_.3, bf16[32,256]{1,0:T(8,128)(2,1)} %refs_2_.1), custom_call_target="tpu_custom_call" | custom-call | tf_op jit(solution)/shard_map/spread/pallas_call | solution.py:212
  11.4 0.0 copy-done.2
  11.4 0.0 copy-done.3
  11.4 0.1 pad_maximum_fusion.2
  11.4 3.1 %all-to-all-done = bf16[4,16,1024]{2,1,0:T(8,128)(2,1)S(1)} async-done(((bf16[4,16,1024]{2,1,0:T(8,128)(2,1)}), bf16[4,16,1024]{2,1,0:T(8,128)(2,1)S(1)}, u32[]{:S(2)}, u32[]{:S(2)}) %all-to-all-start) | async-done | bytes 131104 | tf_op jit(solution)/shard_map/all_to_all | solution.py:222
  14.5 9.8 %all-to-all-start.1 = ((bf16[8,96,256]{2,1,0:T(8,128)(2,1)}), bf16[8,96,256]{2,1,0:T(8,128)(2,1)S(1)}, u32[]{:S(2)}, u32[]{:S(2)}) async-start(bf16[8,96,256]{2,1,0:T(8,128)(2,1)} %spread.1), calls=%async_computation.1 | async-start | bytes 786432 | tf_op jit(solution)/shard_map/all_to_all | solution.py:222
  24.3 0.0 copy-done.4
  24.4 0.1 fusion.11
  24.5 0.0 copy-done.6
  24.5 0.2 multiply_reduce_fusion
  24.7 0.0 copy-done.1
  24.7 0.2 convolution_convert_fusion.2
  25.0 5.8 %all-to-all-done.1 = bf16[8,96,256]{2,1,0:T(8,128)(2,1)S(1)} async-done(((bf16[8,96,256]{2,1,0:T(8,128)(2,1)}), bf16[8,96,256]{2,1,0:T(8,128)(2,1)S(1)}, u32[]{:S(2)}, u32[]{:S(2)}) %all-to-all-start.1) | async-done | bytes 393248 | tf_op jit(solution)/shard_map/all_to_all | solution.py:222
  30.8 29.5 %all_to_all.30 = bf16[128,8,128]{2,1,0:T(8,128)(2,1)S(1)} all-to-all(bf16[128,8,128]{2,1,0:T(8,128)(2,1)S(1)} %bitcast.62), channel_id=1, replica_groups=mesh['z_hi'=4,'z_lo'=2,'y_hi'=4,'y_lo'=2,'c'=2,'x'=4] {'z_hi','z_lo','y_..., dimensions={0} | all-to-all | bytes 524288 | tf_op jit(solution)/shard_map/all_to_all | solution.py:222
  60.3 0.1 slice_bitcast_fusion.9
  60.4 0.2 fusion.9
  60.7 0.1 reshape.92
  60.7 0.1 reshape.93
  60.8 0.3 convolution_convert_fusion.1
  61.1 0.1 pad_maximum_fusion
  61.2 14.4 %all_to_all.31 = bf16[4,384,256]{2,1,0:T(8,128)(2,1)S(1)} all-to-all(bf16[4,384,256]{2,1,0:T(8,128)(2,1)S(1)} %pad_maximum_fusion), channel_id=1, replica_groups=mesh['z_hi'=4,'z_lo'=2,'y_hi'=4,'y_lo'=2,'c'=2,'x'=4] {'x'}, dimensions={0} | all-to-all | bytes 1572864 | tf_op jit(solution)/shard_map/all_to_all | solution.py:222
  75.7 0.3 fusion
  76.0 0.0 copy-done
  76.0 0.3 convolution_convert_fusion
  76.5 12.2 %all_to_all.32 = bf16[4,320,256]{2,1,0:T(8,128)(2,1)S(1)} all-to-all(bf16[4,320,256]{2,1,0:T(8,128)(2,1)S(1)} %pad_maximum_fusion.1), channel_id=1, replica_groups=mesh['z_hi'=4,'z_lo'=2,'y_hi'=4,'y_lo'=2,'c'=2,'x'=4] {'x'}, dimensions={0} | all-to-all | bytes 1310720 | tf_op jit(solution)/shard_map/all_to_all | solution.py:222
  88.6 0.1 slice_reduce_fusion
  88.7 0.1 reshape.95
  88.8 0.0 copy-start.5
  88.8 0.2 convolution_convert_fusion.3
  89.0 0.1 reshape.97
  89.1 0.3 pad_maximum_fusion.3
  89.4 21.9 %all_to_all.33 = bf16[128,4,256]{2,1,0:T(4,128)(2,1)S(1)} all-to-all(bf16[128,4,256]{2,1,0:T(4,128)(2,1)S(1)} %pad_maximum_fusion.3), channel_id=1, replica_groups=mesh['z_hi'=4,'z_lo'=2,'y_hi'=4,'y_lo'=2,'c'=2,'x'=4] {'z_hi','z_lo','y_..., dimensions={0} | all-to-all | bytes 524288 | tf_op jit(solution)/shard_map/all_to_all | solution.py:222
  111.3 0.2 fusion.28
  111.5 0.1 convert_reduce_fusion.1
  111.6 0.1 reshape.98
  111.7 0.1 fusion.30
  111.8 0.7 fusion.20
  (25 shorter events, 0.4 us)
Async XLA Ops:
  0.0 76.0 %copy-start = (bf16[1,128,1024]{2,1,0:T(8,128)(2,1)S(1)}, bf16[1,128,1024]{2,1,0:T(8,128)(2,1)}, u32[]{:S(2)}) copy-start(bf16[1,128,1024]{2,1,0:T(8,128)(2,1)} %param.39) | copy-start | bytes 786436
  0.0 9.7 %copy-start.7 = (f32[16,2]{0,1:T(2,128)S(1)}, f32[16,2]{0,1:T(2,128)}, u32[]{:S(2)}) copy-start(f32[16,2]{0,1:T(2,128)} %param.36) | copy-start | bytes 388
  0.0 9.7 %copy-start.9 = (f32[16]{0:T(128)S(1)}, f32[16]{0:T(128)}, u32[]{:S(2)}) copy-start(f32[16]{0:T(128)} %param.35) | copy-start | bytes 196
  0.0 9.7 %copy-start.8 = (bf16[1024]{0:T(1024)(128)(2,1)S(1)}, bf16[1024]{0:T(1024)(128)(2,1)}, u32[]{:S(2)}) copy-start(bf16[1024]{0:T(1024)(128)(2,1)} %param.43) | copy-start | bytes 6148
  0.0 11.4 %copy-start.2 = (bf16[1,1024,128]{2,1,0:T(8,128)(2,1)S(1)}, bf16[1,1024,128]{2,1,0:T(8,128)(2,1)}, u32[]{:S(2)}) copy-start(bf16[1,1024,128]{2,1,0:T(8,128)(2,1)} %param.38) | copy-start | bytes 786436
  0.0 11.3 %copy-start.3 = (bf16[1,1024,128]{2,1,0:T(8,128)(2,1)S(1)}, bf16[1,1024,128]{2,1,0:T(8,128)(2,1)}, u32[]{:S(2)}) copy-start(bf16[1,1024,128]{2,1,0:T(8,128)(2,1)} %param.37) | copy-start | bytes 786436
  4.9 9.7 %all-to-all-start = ((bf16[4,16,1024]{2,1,0:T(8,128)(2,1)}), bf16[4,16,1024]{2,1,0:T(8,128)(2,1)S(1)}, u32[]{:S(2)}, u32[]{:S(2)}) async-start(bf16[4,16,1024]{2,1,0:T(8,128)(2,1)} %get-tuple-element.19), calls=%async_computation | async-start | bytes 262144 | tf_op jit(solution)/shard_map/all_to_all | solution.py:222
  9.7 14.6 %copy-start.4 = (bf16[16,1024]{1,0:T(8,128)(2,1)S(1)}, bf16[16,1024]{1,0:T(8,128)(2,1)}, u32[]{:S(2)}) copy-start(bf16[16,1024]{1,0:T(8,128)(2,1)} %refs_1_.2) | copy-start | bytes 98308
  9.8 14.7 %copy-start.6 = (f32[1024]{0:T(1024)S(1)}, f32[1024]{0:T(1024)}, u32[]{:S(2)}) copy-start(f32[1024]{0:T(1024)} %param.33) | copy-start | bytes 12292
  9.8 15.0 %copy-start.1 = (bf16[1024,32]{1,0:T(8,128)(2,1)S(1)}, bf16[1024,32]{1,0:T(8,128)(2,1)}, u32[]{:S(2)}) copy-start(bf16[1024,32]{1,0:T(8,128)(2,1)} %get-tuple-element.18) | copy-start | bytes 196612
  14.5 16.2 %all-to-all-start.1 = ((bf16[8,96,256]{2,1,0:T(8,128)(2,1)}), bf16[8,96,256]{2,1,0:T(8,128)(2,1)S(1)}, u32[]{:S(2)}, u32[]{:S(2)}) async-start(bf16[8,96,256]{2,1,0:T(8,128)(2,1)} %spread.1), calls=%async_computation.1 | async-start | bytes 786432 | tf_op jit(solution)/shard_map/all_to_all | solution.py:222
  88.8 22.9 %copy-start.5 = (bf16[32,256]{1,0:T(8,128)(2,1)S(1)}, bf16[32,256]{1,0:T(8,128)(2,1)}, u32[]{:S(2)}) copy-start(bf16[32,256]{1,0:T(8,128)(2,1)} %get-tuple-element.23) | copy-start | bytes 49156

commit v3 on v2

--- a/solution.py
+++ b/solution.py
@@ -74,8 +74,9 @@
 
 
 def mixer_body(near, *refs):
-    rate_ref, sources, targets, buffers = refs[0], refs[1:12], refs[12:15], refs[15:29]
-    sems = refs[29]
+    rate_ref, sources, targets, buffers = refs[0], refs[1:12], refs[12:15], refs[15:26]
+    sems = refs[26]
+    partial_ref, pick_ref, fetch_ref = targets
     (
         hidden_ref,
         gain_ref,
@@ -88,9 +89,6 @@
         value_ref,
         out_w_ref,
         state_ref,
-        partial_ref,
-        pick_ref,
-        fetch_ref,
     ) = buffers
     rows = hidden_ref.shape[0]
     heads = decay_ref.shape[0]
@@ -109,13 +107,10 @@
         )
         for g in range(groups)
     ]
-    puts = [copy_of(buffers[11 + n], targets[n], 14 + n) for n in range(3)]
     for copy in gets[:8] + get_state + gets[8:]:
         copy.start()
     gets[5].wait()
     slots_of(ids_ref, pick_ref, fetch_ref, near, rows)
-    puts[1].start()
-    puts[2].start()
     for copy in gets[:5]:
         copy.wait()
     wide = hidden_ref[...].astype(F32)
@@ -160,9 +155,6 @@
     partial = dot32(head_out, out_w_ref[...]).astype(BF)
     for t in range(partial_ref.shape[0]):
         partial_ref[t] = partial
-    puts[0].start()
-    for copy in puts:
-        copy.wait()
 
 
 def mixer(hidden, state, gain, query, key, value, decay, beta, rate, head_gain, out_w, ids, n_ep, n_tp, near):
@@ -183,17 +175,17 @@
         state.reshape(-1, state.shape[-1]),
     )
     outs = (
-        jax.ShapeDtypeStruct((n_tp, rows, width), BF),
-        jax.ShapeDtypeStruct((n_ep * 8, 2 * rows), BF),
-        jax.ShapeDtypeStruct((ids.size, 2 * n_ep), BF),
+        pltpu.VMEM((n_tp, rows, width), BF),
+        pltpu.VMEM((n_ep * 8, 2 * rows), BF),
+        pltpu.VMEM((ids.size, 2 * n_ep), BF),
     )
     return pl.pallas_call(
         functools.partial(mixer_body, near),
         out_shape=outs,
         in_specs=[smem] + [anywhere] * len(arrays),
-        out_specs=(anywhere,) * len(outs),
-        scratch_shapes=[pltpu.VMEM(a.shape, a.dtype) for a in (*arrays, *outs)]
-        + [pltpu.SemaphoreType.DMA((17,))],
+        out_specs=(pl.BlockSpec(memory_space=pltpu.VMEM),) * len(outs),
+        scratch_shapes=[pltpu.VMEM(a.shape, a.dtype) for a in arrays]
+        + [pltpu.SemaphoreType.DMA((14,))],
         name="mixer",
     )(rate, *arrays)
 
@@ -276,19 +268,11 @@
         n_tp,
         n_near,
     )
-    partials = exchange(copies_out, "x")
-    mix = jnp.sum(partials.astype(F32), axis=0)
-    resid = (hidden_in.astype(F32) + mix).astype(BF)
-    normed2 = rms_scale(resid.astype(F32), ffn_gain, 0.1).astype(BF)
-    own = lax.dynamic_slice_in_dim(normed2, tp_at * quarter, quarter, 1)
-    resid_own = lax.dynamic_slice_in_dim(resid, tp_at * quarter, quarter, 1).astype(F32)
-    gate_wide = branch_gate.astype(F32)
-    branch_dot = jnp.sum(normed2.astype(F32) * gate_wide, axis=1, keepdims=True)
-    branch_weight = jax.nn.sigmoid(branch_dot)
-
-    block = cap + per_near
-    halves = jnp.concatenate([own[:, : quarter // 2], own[:, quarter // 2 :]], axis=0)
-    sent = dot32(pick, halves).astype(BF)
+    fetch, group_share, expert_share, expert_gate, expert_up, branch_gate, tp_at = (
+        lax.optimization_barrier(
+            (fetch, group_share, expert_share, expert_gate, expert_up, branch_gate, tp_at)
+        )
+    )
     n_hid = n_near * hid
     share = n_hid // n_tp
     pairs_near = dense_near[:, :2].reshape(n_tp, -1, 2, hid, quarter)
@@ -299,12 +283,35 @@
         group_share[:, None] * expert_share / jnp.sum(expert_share, axis=1, keepdims=True)
     )
     first_weight, second_weight = route_weight[:, :1], route_weight[:, 1:]
-    sent, both_near, down_near, fetch, expert_both = lax.optimization_barrier(
-        (sent, both_near, down_near, fetch, expert_both)
-    )
-    sent, first_weight, second_weight, branch_weight, resid_own = lax.optimization_barrier(
-        (sent, first_weight, second_weight, branch_weight, resid_own)
-    )
+    gate_wide = branch_gate.astype(F32)
+    half = quarter // 2
+    offset, offset_half = tp_at * quarter, tp_at * quarter + half
+    copies_out, both_near, down_near, fetch, offset, offset_half = lax.optimization_barrier(
+        (copies_out, both_near, down_near, fetch, offset, offset_half)
+    )
+    copies_out, expert_both, first_weight, second_weight, gate_wide = lax.optimization_barrier(
+        (copies_out, expert_both, first_weight, second_weight, gate_wide)
+    )
+    partials = exchange(copies_out, "x")
+    mix = jnp.sum(partials.astype(F32), axis=0)
+    resid = (hidden_in.astype(F32) + mix).astype(BF)
+    normed2 = rms_scale(resid.astype(F32), ffn_gain, 0.1).astype(BF)
+    resid_own = lax.dynamic_slice_in_dim(
+        resid, offset, quarter, 1, allow_negative_indices=False
+    ).astype(F32)
+    branch_dot = jnp.sum(normed2.astype(F32) * gate_wide, axis=1, keepdims=True)
+    branch_weight = jax.nn.sigmoid(branch_dot)
+
+    block = cap + per_near
+    halves = jnp.concatenate(
+        [
+            lax.dynamic_slice_in_dim(normed2, start, half, 1, allow_negative_indices=False)
+            for start in (offset, offset_half)
+        ],
+        axis=0,
+    )
+    sent = dot32(pick, halves).astype(BF)
+    sent, branch_weight, resid_own = lax.optimization_barrier((sent, branch_weight, resid_own))
     arrived = exchange(sent.reshape(n_ep, 8, quarter // 2), EP)
     arrived = arrived.reshape(n_ep, 2, block, quarter // 2)
     arrived = jnp.concatenate([arrived[:, 0], arrived[:, 1]], axis=2)

time: 113 us -> 110 us (0.973)
  blocking collectives: 78.1 us -> 87.1 us
  waiting for transfers between devices: 8.87 us -> 2.1 us
  starting transfers between devices: 14.6 us -> 10.2 us
    all_to_all x4 -> x5, blocking collectives: 78.1 us -> 87.1 us  [exchange(): return lax.all_to_all(blocks, axis, split_axis=0, concat_axis=0, tiled=True)]
    all_to_all x2 -> x1, waiting for transfers between devices: 8.87 us -> 2.1 us  [exchange(): return lax.all_to_all(blocks, axis, split_axis=0, concat_axis=0, tiled=True)]
    all_to_all x2 -> x1, starting transfers between devices: 14.6 us -> 10.2 us  [exchange(): return lax.all_to_all(blocks, axis, split_axis=0, concat_axis=0, tiled=True)]
  transfers between devices with their start and end apart: 2 -> 1, of which waited for: 2 -> 1; matrix products, arithmetic and copies ran while one was open for 1% -> 0% of each run, Pallas kernels for 1% -> 4%
where the time goes in v3:
time: 110 us
  blocking collectives  87.1 us (79%)
  starting transfers between devices  10.2 us (9%)
  Pallas kernels  5.62 us (5%)
  waiting for transfers between devices  2.1 us (2%)
  other arithmetic  2.08 us (2%)
  matrix products  1.42 us (1%)
    all_to_all x5, blocking collectives, exchange(): return lax.all_to_all(blocks, axis, split_axis=0, concat_axis=0, tiled=True)  87.1 us
    all_to_all x1, starting transfers between devices, exchange(): return lax.all_to_all(blocks, axis, split_axis=0, concat_axis=0, tiled=True)  10.2 us
    pallas_call x1, Pallas kernels, mixer(): pl.pallas_call(functools.partial(mixer_body, near), out_shape=outs, in_sp...  4.07 us
  transfers between devices with their start and end apart: 1, of which 1 were waited for; matrix products, arithmetic and copies ran while one was open for 0% of the time, Pallas kernels for 4%

profile of v3, /device:TPU:1, one launch (start us, length us, event | category | flops | bytes accessed | tf_op | source)
XLA Modules:
  0.0 109.8 jit_solution(4027213958519606817)
XLA Ops:
  0.0 0.0 copy-start
  0.0 1.6 %spread.1 = bf16[8,96,256]{2,1,0:T(8,128)(2,1)} custom-call(bf16[32,256]{1,0:T(8,128)(2,1)} %refs_0_.3, bf16[32,256]{1,0:T(8,128)(2,1)} %refs_1_.3, bf16[32,256]{1,0:T(8,128)(2,1)} %refs_2_.1), custom_call_target="tpu_custom_call" | custom-call | tf_op jit(solution)/shard_map/spread/pallas_call | solution.py:204
  1.6 10.2 %all-to-all-start = ((bf16[8,96,256]{2,1,0:T(8,128)(2,1)}), bf16[8,96,256]{2,1,0:T(8,128)(2,1)S(1)}, u32[]{:S(2)}, u32[]{:S(2)}) async-start(bf16[8,96,256]{2,1,0:T(8,128)(2,1)} %spread.1), calls=%async_computation | async-start | bytes 786432 | tf_op jit(solution)/shard_map/all_to_all | solution.py:214
  11.8 0.0 copy-start.5
  11.8 0.0 copy-start.1
  11.8 0.0 copy-start.2
  11.8 0.0 copy-start.7
  11.8 4.1 %mixer.1 = (bf16[4,16,1024]{2,1,0:T(8,128)(2,1)S(1)}, bf16[1024,32]{1,0:T(8,128)(2,1)S(1)}, bf16[32,256]{1,0:T(8,128)(2,1)S(1)}) custom-call(f32[2]{0:T(128)} %refs_0_.2, bf16[16,1024]{1,0:T(8,128)(2,1)} %refs_1_.2, f32[1,1024]{1,0:T(1,128)} %bitcast.71, bf16[2,1024]{1,0:T(2,128)(2,1)} %bitcast.72, bf16[2,1024]{1,0:T(2,128)(2,1)} %bitcast.73, ...), custom_call_target="tpu_custom_call" | custom-call | tf_op jit(solution)/shard_map/mixer/pallas_call | solution.py:182
  15.9 0.0 copy-done.6
  15.9 0.0 copy-done.5
  15.9 0.0 copy-done.1
  15.9 0.0 copy-done.2
  15.9 0.0 copy-start.3
  15.9 0.0 copy-start.4
  16.0 0.1 pad_maximum_fusion.2
  16.0 0.0 copy-done.7
  16.1 2.1 %all-to-all-done = bf16[8,96,256]{2,1,0:T(8,128)(2,1)S(1)} async-done(((bf16[8,96,256]{2,1,0:T(8,128)(2,1)}), bf16[8,96,256]{2,1,0:T(8,128)(2,1)S(1)}, u32[]{:S(2)}, u32[]{:S(2)}) %all-to-all-start) | async-done | bytes 393248 | tf_op jit(solution)/shard_map/all_to_all | solution.py:214
  18.2 7.2 %all_to_all.30 = bf16[4,16,1024]{2,1,0:T(8,128)(2,1)S(1)} all-to-all(bf16[4,16,1024]{2,1,0:T(8,128)(2,1)S(1)} %get-tuple-element.40), channel_id=1, replica_groups=mesh['z_hi'=4,'z_lo'=2,'y_hi'=4,'y_lo'=2,'c'=2,'x'=4] {'x'}, dimensions={0} | all-to-all | bytes 262144 | tf_op jit(solution)/shard_map/all_to_all | solution.py:214
  25.5 0.0 copy-done.3
  25.5 0.1 fusion.11
  25.6 0.1 dynamic-slice_convert_fusion
  25.7 0.0 copy-done.4
  25.7 0.2 multiply_reduce_fusion
  25.9 0.1 constant_dynamic-slice_fusion.1
  26.0 0.2 convolution_convert_fusion.2
  26.2 31.4 %all_to_all.31 = bf16[128,8,128]{2,1,0:T(8,128)(2,1)S(1)} all-to-all(bf16[128,8,128]{2,1,0:T(8,128)(2,1)S(1)} %bitcast.62), channel_id=1, replica_groups=mesh['z_hi'=4,'z_lo'=2,'y_hi'=4,'y_lo'=2,'c'=2,'x'=4] {'z_hi','z_lo','y_..., dimensions={0} | all-to-all | bytes 524288 | tf_op jit(solution)/shard_map/all_to_all | solution.py:214
  57.6 0.1 slice_bitcast_fusion.9
  57.7 0.2 fusion.9
  57.9 0.1 reshape.92
  58.0 0.1 reshape.93
  58.1 0.3 convolution_convert_fusion.1
  58.4 0.1 pad_maximum_fusion
  58.4 14.4 %all_to_all.32 = bf16[4,384,256]{2,1,0:T(8,128)(2,1)S(1)} all-to-all(bf16[4,384,256]{2,1,0:T(8,128)(2,1)S(1)} %pad_maximum_fusion), channel_id=1, replica_groups=mesh['z_hi'=4,'z_lo'=2,'y_hi'=4,'y_lo'=2,'c'=2,'x'=4] {'x'}, dimensions={0} | all-to-all | bytes 1572864 | tf_op jit(solution)/shard_map/all_to_all | solution.py:214
  73.0 0.3 fusion
  73.3 0.0 copy-done
  73.3 0.3 convolution_convert_fusion
  73.7 12.2 %all_to_all.33 = bf16[4,320,256]{2,1,0:T(8,128)(2,1)S(1)} all-to-all(bf16[4,320,256]{2,1,0:T(8,128)(2,1)S(1)} %pad_maximum_fusion.1), channel_id=1, replica_groups=mesh['z_hi'=4,'z_lo'=2,'y_hi'=4,'y_lo'=2,'c'=2,'x'=4] {'x'}, dimensions={0} | all-to-all | bytes 1310720 | tf_op jit(solution)/shard_map/all_to_all | solution.py:214
  85.9 0.1 slice_reduce_fusion
  85.9 0.1 reshape.95
  86.0 0.2 convolution_convert_fusion.3
  86.3 0.1 reshape.97
  86.3 0.3 pad_maximum_fusion.3
  86.6 21.9 %all_to_all.34 = bf16[128,4,256]{2,1,0:T(4,128)(2,1)S(1)} all-to-all(bf16[128,4,256]{2,1,0:T(4,128)(2,1)S(1)} %pad_maximum_fusion.3), channel_id=1, replica_groups=mesh['z_hi'=4,'z_lo'=2,'y_hi'=4,'y_lo'=2,'c'=2,'x'=4] {'z_hi','z_lo','y_..., dimensions={0} | all-to-all | bytes 524288 | tf_op jit(solution)/shard_map/all_to_all | solution.py:214
  108.5 0.2 fusion.28
  108.7 0.1 convert_reduce_fusion.1
  108.9 0.1 reshape.98
  108.9 0.1 fusion.30
  109.1 0.7 fusion.20
  (20 shorter events, 0.4 us)
Async XLA Ops:
  0.0 73.3 %copy-start = (bf16[1,128,1024]{2,1,0:T(8,128)(2,1)S(1)}, bf16[1,128,1024]{2,1,0:T(8,128)(2,1)}, u32[]{:S(2)}) copy-start(bf16[1,128,1024]{2,1,0:T(8,128)(2,1)} %param.39) | copy-start | bytes 786436
  1.6 16.6 %all-to-all-start = ((bf16[8,96,256]{2,1,0:T(8,128)(2,1)}), bf16[8,96,256]{2,1,0:T(8,128)(2,1)S(1)}, u32[]{:S(2)}, u32[]{:S(2)}) async-start(bf16[8,96,256]{2,1,0:T(8,128)(2,1)} %spread.1), calls=%async_computation | async-start | bytes 786432 | tf_op jit(solution)/shard_map/all_to_all | solution.py:214
  11.8 4.1 %copy-start.6 = (bf16[1024]{0:T(1024)(128)(2,1)S(1)}, bf16[1024]{0:T(1024)(128)(2,1)}, u32[]{:S(2)}) copy-start(bf16[1024]{0:T(1024)(128)(2,1)} %param.43) | copy-start | bytes 6148
  11.8 4.1 %copy-start.5 = (f32[16,2]{0,1:T(2,128)S(1)}, f32[16,2]{0,1:T(2,128)}, u32[]{:S(2)}) copy-start(f32[16,2]{0,1:T(2,128)} %param.36) | copy-start | bytes 388
  11.8 4.2 %copy-start.1 = (bf16[1,1024,128]{2,1,0:T(8,128)(2,1)S(1)}, bf16[1,1024,128]{2,1,0:T(8,128)(2,1)}, u32[]{:S(2)}) copy-start(bf16[1,1024,128]{2,1,0:T(8,128)(2,1)} %param.38) | copy-start | bytes 786436
  11.8 4.2 %copy-start.2 = (bf16[1,1024,128]{2,1,0:T(8,128)(2,1)S(1)}, bf16[1,1024,128]{2,1,0:T(8,128)(2,1)}, u32[]{:S(2)}) copy-start(bf16[1,1024,128]{2,1,0:T(8,128)(2,1)} %param.37) | copy-start | bytes 786436
  11.8 4.3 %copy-start.7 = (f32[16]{0:T(128)S(1)}, f32[16]{0:T(128)}, u32[]{:S(2)}) copy-start(f32[16]{0:T(128)} %param.35) | copy-start | bytes 196
  15.9 9.5 %copy-start.3 = (bf16[16,1024]{1,0:T(8,128)(2,1)S(1)}, bf16[16,1024]{1,0:T(8,128)(2,1)}, u32[]{:S(2)}) copy-start(bf16[16,1024]{1,0:T(8,128)(2,1)} %refs_1_.2) | copy-start | bytes 98308
  15.9 9.8 %copy-start.4 = (f32[1024]{0:T(1024)S(1)}, f32[1024]{0:T(1024)}, u32[]{:S(2)}) copy-start(f32[1024]{0:T(1024)} %param.33) | copy-start | bytes 12292

commit v4 on v3

--- a/solution.py
+++ b/solution.py
@@ -268,10 +268,11 @@
         n_tp,
         n_near,
     )
-    fetch, group_share, expert_share, expert_gate, expert_up, branch_gate, tp_at = (
-        lax.optimization_barrier(
-            (fetch, group_share, expert_share, expert_gate, expert_up, branch_gate, tp_at)
-        )
+    fetch, group_share, expert_share, branch_gate, tp_at = lax.optimization_barrier(
+        (fetch, group_share, expert_share, branch_gate, tp_at)
+    )
+    fetch, expert_gate, expert_up, expert_down = lax.optimization_barrier(
+        (fetch, expert_gate, expert_up, expert_down)
     )
     n_hid = n_near * hid
     share = n_hid // n_tp
@@ -279,6 +280,10 @@
     both_near = jnp.swapaxes(pairs_near, 1, 2).reshape(2 * n_hid, quarter)
     down_near = dense_near[:, 2].reshape(n_hid, quarter)
     expert_both = jnp.concatenate([expert_gate[0], expert_up[0]], axis=1)
+    down_blocks = [expert_down[0, :, t * quarter : (t + 1) * quarter] for t in range(n_tp)]
+    packed = jnp.concatenate([expert_both, *down_blocks], axis=0)
+    swap = [(t, t ^ 1) for t in range(n_tp)]
+    from_partner = lax.ppermute(packed, "x", swap)
     route_weight = (
         group_share[:, None] * expert_share / jnp.sum(expert_share, axis=1, keepdims=True)
     )
@@ -320,26 +325,39 @@
 
     contract = (((1,), (1,)), ((), ()))
     pre = lax.dot_general(both_near, dense_rows, contract, preferred_element_type=F32)
-    pre = pre.astype(BF).reshape(n_tp, 2 * share, -1)
-    moe_copies = jnp.broadcast_to(moe_rows, (n_tp, *moe_rows.shape))
-    first = exchange(jnp.concatenate([moe_copies, pre], axis=1), "x")
-
-    n_rows = n_ep * cap
-    pre_sum = jnp.sum(first[:, n_rows:].astype(F32), axis=0)
+    pre = pre.astype(BF)
+    pre = pre.reshape(n_tp, 2 * share, -1)
+    served = n_ep * cap // 2
+    moe_halves = jnp.concatenate([moe_rows] * (n_tp // 2), axis=0).reshape(n_tp, served, quarter)
+    partner_both = from_partner[:width]
+    units = expert_down.shape[1]
+    partner_down = jnp.concatenate(
+        [from_partner[width + t * units : width + (t + 1) * units] for t in range(n_tp)], axis=1
+    )
+    first = jnp.concatenate([moe_halves, pre], axis=1)
+    first, partner_both, partner_down = lax.optimization_barrier(
+        (first, partner_both, partner_down)
+    )
+    first = exchange(first, "x")
+
+    pre_sum = jnp.sum(first[:, served:].astype(F32), axis=0)
     dense_hidden = (jax.nn.silu(pre_sum[:share]) * pre_sum[share:]).astype(BF)
-    full_rows = jnp.concatenate([first[t, :n_rows] for t in range(n_tp)], axis=1)
-    both_pre = dot32(full_rows, expert_both)
-    wide = both_pre.shape[1] // 2
-    hidden = (jax.nn.silu(both_pre[:, :wide]) * both_pre[:, wide:]).astype(BF)
-    expert_part = dot32(hidden, expert_down[0]).astype(BF)
+    full_rows = jnp.concatenate([first[t, :served] for t in range(n_tp)], axis=1)
+    expert_part = 0.0
+    for w_both, w_down in ((expert_both, expert_down[0]), (partner_both, partner_down)):
+        both_pre = dot32(full_rows, w_both)
+        hidden = (jax.nn.silu(both_pre[:, :units]) * both_pre[:, units:]).astype(BF)
+        expert_part = expert_part + dot32(hidden, w_down)
+    expert_part = expert_part.astype(BF)
     part_blocks = jnp.stack(
         [expert_part[:, t * quarter : (t + 1) * quarter] for t in range(n_tp)], axis=0
     )
     hidden_copies = jnp.broadcast_to(dense_hidden, (n_tp, *dense_hidden.shape))
     second = exchange(jnp.concatenate([part_blocks, hidden_copies], axis=1), "x")
 
-    expert_out = jnp.sum(second[:, :n_rows].astype(F32), axis=0).astype(BF)
-    all_hidden = second[:, n_rows:].reshape(n_hid, -1)
+    by_pair = second[:, :served].astype(F32).reshape(n_tp // 2, 2 * served, quarter)
+    expert_out = jnp.sum(by_pair, axis=0).astype(BF)
+    all_hidden = second[:, served:].reshape(n_hid, -1)
     dense_out = lax.dot_general(
         all_hidden, down_near, (((0,), (0,)), ((), ())), preferred_element_type=F32
     ).astype(BF)

time: 110 us -> 107 us (0.973)
  blocking collectives: 87.1 us -> 43 us
  starting transfers between devices: 10.2 us -> 33.2 us
  waiting for transfers between devices: 2.1 us -> 18 us
    all_to_all x5 -> x3, blocking collectives: 87.1 us -> 43 us  [exchange(): return lax.all_to_all(blocks, axis, split_axis=0, concat_axis=0, tiled=True)]
    all_to_all x1 -> x3, starting transfers between devices: 10.2 us -> 29.9 us  [exchange(): return lax.all_to_all(blocks, axis, split_axis=0, concat_axis=0, tiled=True)]
    all_to_all x1 -> x3, waiting for transfers between devices: 2.1 us -> 18 us  [exchange(): return lax.all_to_all(blocks, axis, split_axis=0, concat_axis=0, tiled=True)]
    ppermute x0 -> x1, starting transfers between devices: none -> 3.33 us  [local(): from_partner = lax.ppermute(packed, 'x', swap)]
  transfers between devices with their start and end apart: 1 -> 4, of which waited for: 1 -> 3; matrix products, arithmetic and copies ran while one was open for 0% -> 2% of each run, Pallas kernels for 4% -> 4%
where the time goes in v4:
time: 107 us; the launch traced here: 106 us
  blocking collectives  43 us (40%)
  starting transfers between devices  33.2 us (31%)
  waiting for transfers between devices  18 us (17%)
  Pallas kernels  6.23 us (6%)
  matrix products  2.43 us (2%)
  other arithmetic  2.06 us (2%)
    all_to_all x3, blocking collectives, exchange(): return lax.all_to_all(blocks, axis, split_axis=0, concat_axis=0, tiled=True)  43 us
    all_to_all x3, starting transfers between devices, exchange(): return lax.all_to_all(blocks, axis, split_axis=0, concat_axis=0, tiled=True)  29.9 us
    all_to_all x3, waiting for transfers between devices, exchange(): return lax.all_to_all(blocks, axis, split_axis=0, concat_axis=0, tiled=True)  18 us
    pallas_call x1, Pallas kernels, mixer(): pl.pallas_call(functools.partial(mixer_body, near), out_shape=outs, in_sp...  4.72 us
    ppermute x1, starting transfers between devices, local(): from_partner = lax.ppermute(packed, 'x', swap)  3.33 us
  transfers between devices with their start and end apart: 4, of which 3 were waited for; matrix products, arithmetic and copies ran while one was open for 2% of the time, Pallas kernels for 4%

profile of v4, /device:TPU:1, one launch (start us, length us, event | category | flops | bytes accessed | tf_op | source)
XLA Modules:
  0.0 106.3 jit_solution(10713374819467753487)
XLA Ops:
  0.0 1.5 %spread.1 = bf16[8,96,256]{2,1,0:T(8,128)(2,1)} custom-call(bf16[32,256]{1,0:T(8,128)(2,1)} %refs_0_.3, bf16[32,256]{1,0:T(8,128)(2,1)} %refs_1_.3, bf16[32,256]{1,0:T(8,128)(2,1)} %refs_2_.1), custom_call_target="tpu_custom_call" | custom-call | tf_op jit(solution)/shard_map/spread/pallas_call | solution.py:204
  1.5 10.2 %all-to-all-start = ((bf16[8,96,256]{2,1,0:T(8,128)(2,1)}), bf16[8,96,256]{2,1,0:T(8,128)(2,1)S(1)}, u32[]{:S(2)}, u32[]{:S(2)}) async-start(bf16[8,96,256]{2,1,0:T(8,128)(2,1)} %spread.1), calls=%async_computation | async-start | bytes 786432 | tf_op jit(solution)/shard_map/all_to_all | solution.py:214
  11.7 0.0 copy-start.3
  11.7 0.0 copy-start.7
  11.7 0.0 copy-start
  11.8 4.7 %mixer.1 = (bf16[4,16,1024]{2,1,0:T(8,128)(2,1)}, bf16[1024,32]{1,0:T(8,128)(2,1)S(1)}, bf16[32,256]{1,0:T(8,128)(2,1)S(1)}) custom-call(f32[2]{0:T(128)} %refs_0_.2, bf16[16,1024]{1,0:T(8,128)(2,1)} %refs_1_.2, f32[1,1024]{1,0:T(1,128)} %bitcast.86, bf16[2,1024]{1,0:T(2,128)(2,1)} %bitcast.87, bf16[2,1024]{1,0:T(2,128)(2,1)} %bitcast.88, ...), custom_call_target="tpu_custom_call" | custom-call | tf_op jit(solution)/shard_map/mixer/pallas_call | solution.py:182
  16.5 0.0 copy-start.4
  16.5 0.0 copy-start.5
  16.5 0.0 copy-done.6
  16.5 0.0 copy-done.8
  16.6 0.0 copy-done.2
  16.6 0.0 copy-done.3
  16.6 0.1 constant_dynamic-update-slice_fusion
  16.7 0.0 copy-done
  16.8 1.4 %all-to-all-done = bf16[8,96,256]{2,1,0:T(8,128)(2,1)S(1)} async-done(((bf16[8,96,256]{2,1,0:T(8,128)(2,1)}), bf16[8,96,256]{2,1,0:T(8,128)(2,1)S(1)}, u32[]{:S(2)}, u32[]{:S(2)}) %all-to-all-start) | async-done | bytes 393248 | tf_op jit(solution)/shard_map/all_to_all | solution.py:214
  18.2 3.3 %all-to-all-start.1 = ((bf16[4,16,1024]{2,1,0:T(8,128)(2,1)}), bf16[4,16,1024]{2,1,0:T(8,128)(2,1)S(1)}, u32[]{:S(2)}, u32[]{:S(2)}) async-start(bf16[4,16,1024]{2,1,0:T(8,128)(2,1)} %get-tuple-element.46), calls=%async_computation.1 | async-start | bytes 262144 | tf_op jit(solution)/shard_map/all_to_all | solution.py:214
  21.5 3.3 %collective-permute-start = (bf16[1536,256]{1,0:T(8,128)(2,1)S(1)}, bf16[1536,256]{1,0:T(8,128)(2,1)S(1)}, u32[]{:S(2)}, u32[]{:S(2)}) collective-permute-start(bf16[1536,256]{1,0:T(8,128)(2,1)S(1)} %bitcast_dynamic-update-slice_fusion), channel_id=1, source_target_pairs={{0,1},{1,0},{2,3},{3,2},{4,5},{5,4},{6,7},{7,6},{8,9},{9,8},{10,11... | collective-permute-start | bytes 2359304 | tf_op jit(solution)/shard_map/ppermute | solution.py:286
  24.9 1.4 %all-to-all-done.1 = bf16[4,16,1024]{2,1,0:T(8,128)(2,1)S(1)} async-done(((bf16[4,16,1024]{2,1,0:T(8,128)(2,1)}), bf16[4,16,1024]{2,1,0:T(8,128)(2,1)S(1)}, u32[]{:S(2)}, u32[]{:S(2)}) %all-to-all-start.1) | async-done | bytes 131104 | tf_op jit(solution)/shard_map/all_to_all | solution.py:214
  26.4 0.1 fusion.4
  26.5 0.2 multiply_reduce_fusion
  26.7 0.1 constant_dynamic-slice_fusion.1
  26.8 0.1 dynamic-slice_convert_fusion
  26.9 0.9 convolution_convert_fusion.1
  27.8 16.4 %all-to-all-start.2 = ((bf16[128,8,128]{2,1,0:T(8,128)(2,1)}), bf16[128,8,128]{2,1,0:T(8,128)(2,1)S(1)}, u32[]{:S(2)}, u32[]{:S(2)}) async-start(bf16[128,8,128]{2,1,0:T(8,128)(2,1)} %bitcast.14), calls=%async_computation.2 | async-start | bytes 524288 | tf_op jit(solution)/shard_map/all_to_all | solution.py:214
  44.1 0.0 collective-permute-done
  44.2 15.2 %all-to-all-done.2 = bf16[128,8,128]{2,1,0:T(8,128)(2,1)S(1)} async-done(((bf16[128,8,128]{2,1,0:T(8,128)(2,1)}), bf16[128,8,128]{2,1,0:T(8,128)(2,1)S(1)}, u32[]{:S(2)}, u32[]{:S(2)}) %all-to-all-start.2) | async-done | bytes 262176 | tf_op jit(solution)/shard_map/all_to_all | solution.py:214
  59.4 0.1 slice_bitcast_fusion.1
  59.5 0.2 fusion.3
  59.7 0.1 reshape.103
  59.8 0.1 reshape.101
  59.8 0.3 convolution_convert_fusion
  60.2 0.0 slice-start
  60.2 11.7 %all_to_all.30 = bf16[4,256,256]{2,1,0:T(8,128)(2,1)S(1)} all-to-all(bf16[4,256,256]{2,1,0:T(8,128)(2,1)S(1)} %pad_maximum_fusion.1), channel_id=1, replica_groups=mesh['z_hi'=4,'z_lo'=2,'y_hi'=4,'y_lo'=2,'c'=2,'x'=4] {'x'}, dimensions={0} | all-to-all | bytes 1048576 | tf_op jit(solution)/shard_map/all_to_all | solution.py:214
  72.0 0.2 fusion.11
  72.3 0.2 fusion.1
  72.5 0.2 fusion.10
  72.7 0.2 fusion
  73.0 9.3 %all_to_all.31 = bf16[4,192,256]{2,1,0:T(8,128)(2,1)S(1)} all-to-all(bf16[4,192,256]{2,1,0:T(8,128)(2,1)S(1)} %pad_maximum_fusion.2), channel_id=1, replica_groups=mesh['z_hi'=4,'z_lo'=2,'y_hi'=4,'y_lo'=2,'c'=2,'x'=4] {'x'}, dimensions={0} | all-to-all | bytes 786432 | tf_op jit(solution)/shard_map/all_to_all | solution.py:214
  82.4 0.2 convolution_convert_fusion.2
  82.6 0.1 reshape.108
  82.7 0.1 convert_element_type.76
  82.8 0.3 pad_maximum_fusion.6
  83.1 21.9 %all_to_all.32 = bf16[128,4,256]{2,1,0:T(4,128)(2,1)S(1)} all-to-all(bf16[128,4,256]{2,1,0:T(4,128)(2,1)S(1)} %pad_maximum_fusion.6), channel_id=1, replica_groups=mesh['z_hi'=4,'z_lo'=2,'y_hi'=4,'y_lo'=2,'c'=2,'x'=4] {'z_hi','z_lo','y_..., dimensions={0} | all-to-all | bytes 524288 | tf_op jit(solution)/shard_map/all_to_all | solution.py:214
  105.0 0.2 fusion.30
  105.2 0.1 reshape.109
  105.3 0.1 convert_reduce_fusion.1
  105.4 0.1 fusion.32
  105.6 0.7 fusion.19
  (37 shorter events, 0.5 us)
Async XLA Ops:
  1.5 16.6 %all-to-all-start = ((bf16[8,96,256]{2,1,0:T(8,128)(2,1)}), bf16[8,96,256]{2,1,0:T(8,128)(2,1)S(1)}, u32[]{:S(2)}, u32[]{:S(2)}) async-start(bf16[8,96,256]{2,1,0:T(8,128)(2,1)} %spread.1), calls=%async_computation | async-start | bytes 786432 | tf_op jit(solution)/shard_map/all_to_all | solution.py:214
  11.7 4.8 %copy-start.6 = (f32[16,2]{0,1:T(2,128)S(1)}, f32[16,2]{0,1:T(2,128)}, u32[]{:S(2)}) copy-start(f32[16,2]{0,1:T(2,128)} %param.36) | copy-start | bytes 388
  11.7 4.8 %copy-start.8 = (f32[16]{0:T(128)S(1)}, f32[16]{0:T(128)}, u32[]{:S(2)}) copy-start(f32[16]{0:T(128)} %param.35) | copy-start | bytes 196
  11.7 4.9 %copy-start.2 = (bf16[1,1024,128]{2,1,0:T(8,128)(2,1)S(1)}, bf16[1,1024,128]{2,1,0:T(8,128)(2,1)}, u32[]{:S(2)}) copy-start(bf16[1,1024,128]{2,1,0:T(8,128)(2,1)} %param.38) | copy-start | bytes 786436
  11.7 4.9 %copy-start.3 = (bf16[1,1024,128]{2,1,0:T(8,128)(2,1)S(1)}, bf16[1,1024,128]{2,1,0:T(8,128)(2,1)}, u32[]{:S(2)}) copy-start(bf16[1,1024,128]{2,1,0:T(8,128)(2,1)} %param.37) | copy-start | bytes 786436
  11.7 4.9 %copy-start.7 = (bf16[1024]{0:T(1024)(128)(2,1)S(1)}, bf16[1024]{0:T(1024)(128)(2,1)}, u32[]{:S(2)}) copy-start(bf16[1024]{0:T(1024)(128)(2,1)} %param.43) | copy-start | bytes 6148
  11.7 5.0 %copy-start = (bf16[1,128,1024]{2,1,0:T(8,128)(2,1)S(1)}, bf16[1,128,1024]{2,1,0:T(8,128)(2,1)}, u32[]{:S(2)}) copy-start(bf16[1,128,1024]{2,1,0:T(8,128)(2,1)} %param.39) | copy-start | bytes 786436
  16.5 9.9 %copy-start.4 = (bf16[16,1024]{1,0:T(8,128)(2,1)S(1)}, bf16[16,1024]{1,0:T(8,128)(2,1)}, u32[]{:S(2)}) copy-start(bf16[16,1024]{1,0:T(8,128)(2,1)} %refs_1_.2) | copy-start | bytes 98308
  16.5 10.0 %copy-start.5 = (f32[1024]{0:T(1024)S(1)}, f32[1024]{0:T(1024)}, u32[]{:S(2)}) copy-start(f32[1024]{0:T(1024)} %param.33) | copy-start | bytes 12292
  18.2 8.1 %all-to-all-start.1 = ((bf16[4,16,1024]{2,1,0:T(8,128)(2,1)}), bf16[4,16,1024]{2,1,0:T(8,128)(2,1)S(1)}, u32[]{:S(2)}, u32[]{:S(2)}) async-start(bf16[4,16,1024]{2,1,0:T(8,128)(2,1)} %get-tuple-element.46), calls=%async_computation.1 | async-start | bytes 262144 | tf_op jit(solution)/shard_map/all_to_all | solution.py:214
  21.5 22.6 %collective-permute-start = (bf16[1536,256]{1,0:T(8,128)(2,1)S(1)}, bf16[1536,256]{1,0:T(8,128)(2,1)S(1)}, u32[]{:S(2)}, u32[]{:S(2)}) collective-permute-start(bf16[1536,256]{1,0:T(8,128)(2,1)S(1)} %bitcast_dynamic-update-slice_fusion), channel_id=1, source_target_pairs={{0,1},{1,0},{2,3},{3,2},{4,5},{5,4},{6,7},{7,6},{8,9},{9,8},{10,11... | collective-permute-start | bytes 2359304 | tf_op jit(solution)/shard_map/ppermute | solution.py:286
  27.8 31.6 %all-to-all-start.2 = ((bf16[128,8,128]{2,1,0:T(8,128)(2,1)}), bf16[128,8,128]{2,1,0:T(8,128)(2,1)S(1)}, u32[]{:S(2)}, u32[]{:S(2)}) async-start(bf16[128,8,128]{2,1,0:T(8,128)(2,1)} %bitcast.14), calls=%async_computation.2 | async-start | bytes 524288 | tf_op jit(solution)/shard_map/all_to_all | solution.py:214
  44.1 16.0 %copy-start.1 = (bf16[1536,256]{1,0:T(8,128)(2,1)}, bf16[1536,256]{1,0:T(8,128)(2,1)S(1)}, u32[]{:S(2)}) copy-start(bf16[1536,256]{1,0:T(8,128)(2,1)S(1)} %collective-permute-done) | copy-start | bytes 2359300
  60.2 12.3 %slice-start = ((bf16[1536,256]{1,0:T(8,128)(2,1)}), bf16[1024,256]{1,0:T(8,128)(2,1)S(1)}, s32[]{:S(2)}) async-start(bf16[1536,256]{1,0:T(8,128)(2,1)} %copy-done.1), calls=%async_computation.6 | async-start | bytes 1048576 | tf_op jit(solution)/shard_map/slice | solution.py:332

commit v5 on v4

--- a/solution.py
+++ b/solution.py
@@ -335,20 +335,20 @@
         [from_partner[width + t * units : width + (t + 1) * units] for t in range(n_tp)], axis=1
     )
     first = jnp.concatenate([moe_halves, pre], axis=1)
-    first, partner_both, partner_down = lax.optimization_barrier(
-        (first, partner_both, partner_down)
-    )
+    w_both = jnp.concatenate([expert_both, partner_both], axis=1)
+    w_down = jnp.concatenate([expert_down[0], partner_down], axis=0)
+    first, w_both, w_down = lax.optimization_barrier((first, w_both, w_down))
     first = exchange(first, "x")
 
     pre_sum = jnp.sum(first[:, served:].astype(F32), axis=0)
     dense_hidden = (jax.nn.silu(pre_sum[:share]) * pre_sum[share:]).astype(BF)
     full_rows = jnp.concatenate([first[t, :served] for t in range(n_tp)], axis=1)
-    expert_part = 0.0
-    for w_both, w_down in ((expert_both, expert_down[0]), (partner_both, partner_down)):
-        both_pre = dot32(full_rows, w_both)
-        hidden = (jax.nn.silu(both_pre[:, :units]) * both_pre[:, units:]).astype(BF)
-        expert_part = expert_part + dot32(hidden, w_down)
-    expert_part = expert_part.astype(BF)
+    both_pre = dot32(full_rows, w_both)
+    gates = [both_pre[:, n * units : (n + 1) * units] for n in range(4)]
+    hidden = jnp.concatenate(
+        [jax.nn.silu(gates[0]) * gates[1], jax.nn.silu(gates[2]) * gates[3]], axis=1
+    ).astype(BF)
+    expert_part = dot32(hidden, w_down).astype(BF)
     part_blocks = jnp.stack(
         [expert_part[:, t * quarter : (t + 1) * quarter] for t in range(n_tp)], axis=0
     )

time: 107 us -> 107 us (level)
  local copies, waits for them, and re-layouts: 0.92 us -> 4.01 us
  starting transfers between devices: 33.2 us -> 31 us
  waiting for transfers between devices: 18 us -> 15.9 us
  other arithmetic: 2.06 us -> 4.11 us
    all_to_all x3, starting transfers between devices: 29.9 us -> 27.7 us  [exchange(): return lax.all_to_all(blocks, axis, split_axis=0, concat_axis=0, tiled=True)]
    all_to_all x3, waiting for transfers between devices: 18 us -> 15.9 us  [exchange(): return lax.all_to_all(blocks, axis, split_axis=0, concat_axis=0, tiled=True)]
    unnamed x21 -> x27, local copies, waits for them, and re-layouts: 0.08 us -> 1.94 us
  transfers between devices with their start and end apart: 4 -> 4, of which waited for: 3 -> 2; matrix products, arithmetic and copies ran while one was open for 2% -> 6% of each run, Pallas kernels for 4% -> 4%
where the time goes in v5:
time: 107 us
  blocking collectives  42.9 us (40%)
  starting transfers between devices  31 us (29%)
  waiting for transfers between devices  15.9 us (15%)
  Pallas kernels  6.25 us (6%)
  other arithmetic  4.11 us (4%)
  local copies, waits for them, and re-layouts  4.01 us (4%)
  matrix products  2.05 us (2%)
    all_to_all x3, blocking collectives, exchange(): return lax.all_to_all(blocks, axis, split_axis=0, concat_axis=0, tiled=True)  42.9 us
    all_to_all x3, starting transfers between devices, exchange(): return lax.all_to_all(blocks, axis, split_axis=0, concat_axis=0, tiled=True)  27.7 us
    all_to_all x3, waiting for transfers between devices, exchange(): return lax.all_to_all(blocks, axis, split_axis=0, concat_axis=0, tiled=True)  15.9 us
    pallas_call x1, Pallas kernels, mixer(): pl.pallas_call(functools.partial(mixer_body, near), out_shape=outs, in_sp...  4.72 us
    ppermute x1, starting transfers between devices, local(): from_partner = lax.ppermute(packed, 'x', swap)  3.32 us
  transfers between devices with their start and end apart: 4, of which 2 were waited for; matrix products, arithmetic and copies ran while one was open for 6% of the time, Pallas kernels for 4%

profile of v5, /device:TPU:1, one launch (start us, length us, event | category | flops | bytes accessed | tf_op | source)
XLA Modules:
  0.0 106.6 jit_solution(9472164818681296571)
XLA Ops:
  0.0 1.5 %spread.1 = bf16[8,96,256]{2,1,0:T(8,128)(2,1)} custom-call(bf16[32,256]{1,0:T(8,128)(2,1)} %refs_0_.3, bf16[32,256]{1,0:T(8,128)(2,1)} %refs_1_.3, bf16[32,256]{1,0:T(8,128)(2,1)} %refs_2_.1), custom_call_target="tpu_custom_call" | custom-call | tf_op jit(solution)/shard_map/spread/pallas_call | solution.py:204
  1.5 10.2 %all-to-all-start = ((bf16[8,96,256]{2,1,0:T(8,128)(2,1)}), bf16[8,96,256]{2,1,0:T(8,128)(2,1)S(1)}, u32[]{:S(2)}, u32[]{:S(2)}) async-start(bf16[8,96,256]{2,1,0:T(8,128)(2,1)} %spread.1), calls=%async_computation | async-start | bytes 786432 | tf_op jit(solution)/shard_map/all_to_all | solution.py:214
  11.7 0.0 copy-start.2
  11.7 0.0 copy-start.9
  11.8 0.0 copy-start
  11.8 4.7 %mixer.1 = (bf16[4,16,1024]{2,1,0:T(8,128)(2,1)}, bf16[1024,32]{1,0:T(8,128)(2,1)S(1)}, bf16[32,256]{1,0:T(8,128)(2,1)S(1)}) custom-call(f32[2]{0:T(128)} %refs_0_.2, bf16[16,1024]{1,0:T(8,128)(2,1)} %refs_1_.2, f32[1,1024]{1,0:T(1,128)} %bitcast.84, bf16[2,1024]{1,0:T(2,128)(2,1)} %bitcast.85, bf16[2,1024]{1,0:T(2,128)(2,1)} %bitcast.86, ...), custom_call_target="tpu_custom_call" | custom-call | tf_op jit(solution)/shard_map/mixer/pallas_call | solution.py:182
  16.5 0.0 copy-start.3
  16.5 0.0 copy-start.5
  16.6 0.6 fusion.31
  17.2 0.9 constant_dynamic-update-slice_fusion
  18.0 0.6 bitcast_dynamic-update-slice_fusion.3
  18.7 0.6 bitcast_dynamic-update-slice_fusion.2
  19.3 0.6 bitcast_dynamic-update-slice_fusion.1
  20.0 3.3 %all-to-all-start.1 = ((bf16[4,16,1024]{2,1,0:T(8,128)(2,1)}), bf16[4,16,1024]{2,1,0:T(8,128)(2,1)S(1)}, u32[]{:S(2)}, u32[]{:S(2)}) async-start(bf16[4,16,1024]{2,1,0:T(8,128)(2,1)} %get-tuple-element.46), calls=%async_computation.1 | async-start | bytes 262144 | tf_op jit(solution)/shard_map/all_to_all | solution.py:214
  23.3 0.6 bitcast_dynamic-update-slice_fusion
  23.9 3.3 %collective-permute-start = (bf16[1536,256]{1,0:T(8,128)(2,1)}, bf16[1536,256]{1,0:T(8,128)(2,1)S(1)}, u32[]{:S(2)}, u32[]{:S(2)}) collective-permute-start(bf16[1536,256]{1,0:T(8,128)(2,1)} %bitcast_dynamic-update-slice_fusion), channel_id=1, source_target_pairs={{0,1},{1,0},{2,3},{3,2},{4,5},{5,4},{6,7},{7,6},{8,9},{9,8},{10,11... | collective-permute-start | bytes 2359304 | tf_op jit(solution)/shard_map/ppermute | solution.py:286
  27.3 0.9 all-to-all-done.1
  28.2 0.1 fusion.9
  28.4 0.2 multiply_reduce_fusion
  28.6 0.1 constant_dynamic-slice_fusion.1
  28.7 0.7 dynamic-slice_convert_fusion
  29.3 0.5 divide_bitcast_fusion
  29.9 0.9 convolution_convert_fusion.2
  30.8 14.2 %all-to-all-start.2 = ((bf16[128,8,128]{2,1,0:T(8,128)(2,1)}), bf16[128,8,128]{2,1,0:T(8,128)(2,1)S(1)}, u32[]{:S(2)}, u32[]{:S(2)}) async-start(bf16[128,8,128]{2,1,0:T(8,128)(2,1)} %bitcast.14), calls=%async_computation.2 | async-start | bytes 524288 | tf_op jit(solution)/shard_map/all_to_all | solution.py:214
  45.0 0.0 collective-permute-done
  45.1 0.1 maximum_maximum_fusion
  45.1 0.1 pad_maximum_fusion
  45.2 15.0 %all-to-all-done.2 = bf16[128,8,128]{2,1,0:T(8,128)(2,1)S(1)} async-done(((bf16[128,8,128]{2,1,0:T(8,128)(2,1)}), bf16[128,8,128]{2,1,0:T(8,128)(2,1)S(1)}, u32[]{:S(2)}, u32[]{:S(2)}) %all-to-all-start.2) | async-done | bytes 262176 | tf_op jit(solution)/shard_map/all_to_all | solution.py:214
  60.2 0.1 slice_bitcast_fusion.1
  60.3 0.2 fusion.8
  60.6 0.1 reshape.101
  60.6 0.1 reshape.103
  60.7 0.3 convolution_convert_fusion.1
  61.0 11.6 %all_to_all.30 = bf16[4,256,256]{2,1,0:T(8,128)(2,1)S(1)} all-to-all(bf16[4,256,256]{2,1,0:T(8,128)(2,1)S(1)} %pad_maximum_fusion.2), channel_id=1, replica_groups=mesh['z_hi'=4,'z_lo'=2,'y_hi'=4,'y_lo'=2,'c'=2,'x'=4] {'x'}, dimensions={0} | all-to-all | bytes 1048576 | tf_op jit(solution)/shard_map/all_to_all | solution.py:214
  72.7 0.3 fusion
  73.1 0.2 convolution_convert_fusion
  73.4 9.3 %all_to_all.31 = bf16[4,192,256]{2,1,0:T(8,128)(2,1)S(1)} all-to-all(bf16[4,192,256]{2,1,0:T(8,128)(2,1)S(1)} %pad_maximum_fusion.3), channel_id=1, replica_groups=mesh['z_hi'=4,'z_lo'=2,'y_hi'=4,'y_lo'=2,'c'=2,'x'=4] {'x'}, dimensions={0} | all-to-all | bytes 786432 | tf_op jit(solution)/shard_map/all_to_all | solution.py:214
  82.8 0.1 convert_element_type.69
  82.9 0.2 convolution_convert_fusion.3
  83.1 0.1 reshape.108
  83.2 0.3 pad_maximum_fusion.5
  83.5 22.0 %all_to_all.32 = bf16[128,4,256]{2,1,0:T(4,128)(2,1)S(1)} all-to-all(bf16[128,4,256]{2,1,0:T(4,128)(2,1)S(1)} %pad_maximum_fusion.5), channel_id=1, replica_groups=mesh['z_hi'=4,'z_lo'=2,'y_hi'=4,'y_lo'=2,'c'=2,'x'=4] {'z_hi','z_lo','y_..., dimensions={0} | all-to-all | bytes 524288 | tf_op jit(solution)/shard_map/all_to_all | solution.py:214
  105.4 0.2 fusion.30
  105.6 0.1 convert_reduce_fusion.1
  105.7 0.1 reshape.109
  105.8 0.1 fusion.32
  105.9 0.0 copy-done.8
  106.0 0.7 fusion.21
  (42 shorter events, 0.5 us)
Async XLA Ops:
  1.5 18.4 %all-to-all-start = ((bf16[8,96,256]{2,1,0:T(8,128)(2,1)}), bf16[8,96,256]{2,1,0:T(8,128)(2,1)S(1)}, u32[]{:S(2)}, u32[]{:S(2)}) async-start(bf16[8,96,256]{2,1,0:T(8,128)(2,1)} %spread.1), calls=%async_computation | async-start | bytes 786432 | tf_op jit(solution)/shard_map/all_to_all | solution.py:214
  11.7 4.8 %copy-start.6 = (f32[16,2]{0,1:T(2,128)S(1)}, f32[16,2]{0,1:T(2,128)}, u32[]{:S(2)}) copy-start(f32[16,2]{0,1:T(2,128)} %param.36) | copy-start | bytes 388
  11.7 4.8 %copy-start.11 = (f32[16]{0:T(128)S(1)}, f32[16]{0:T(128)}, u32[]{:S(2)}) copy-start(f32[16]{0:T(128)} %param.35) | copy-start | bytes 196
  11.7 5.4 %copy-start.1 = (bf16[1,1024,128]{2,1,0:T(8,128)(2,1)S(1)}, bf16[1,1024,128]{2,1,0:T(8,128)(2,1)}, u32[]{:S(2)}) copy-start(bf16[1,1024,128]{2,1,0:T(8,128)(2,1)} %param.38) | copy-start | bytes 786436
  11.7 5.4 %copy-start.2 = (bf16[1,1024,128]{2,1,0:T(8,128)(2,1)S(1)}, bf16[1,1024,128]{2,1,0:T(8,128)(2,1)}, u32[]{:S(2)}) copy-start(bf16[1,1024,128]{2,1,0:T(8,128)(2,1)} %param.37) | copy-start | bytes 786436
  11.7 6.3 %copy-start.9 = (bf16[1024]{0:T(1024)(128)(2,1)S(1)}, bf16[1024]{0:T(1024)(128)(2,1)}, u32[]{:S(2)}) copy-start(bf16[1024]{0:T(1024)(128)(2,1)} %param.43) | copy-start | bytes 6148
  11.8 6.3 %copy-start = (bf16[1,128,1024]{2,1,0:T(8,128)(2,1)S(1)}, bf16[1,128,1024]{2,1,0:T(8,128)(2,1)}, u32[]{:S(2)}) copy-start(bf16[1,128,1024]{2,1,0:T(8,128)(2,1)} %param.39) | copy-start | bytes 786436
  16.5 11.7 %copy-start.3 = (bf16[16,1024]{1,0:T(8,128)(2,1)S(1)}, bf16[16,1024]{1,0:T(8,128)(2,1)}, u32[]{:S(2)}) copy-start(bf16[16,1024]{1,0:T(8,128)(2,1)} %refs_1_.2) | copy-start | bytes 98308
  16.5 11.9 %copy-start.5 = (f32[1024]{0:T(1024)S(1)}, f32[1024]{0:T(1024)}, u32[]{:S(2)}) copy-start(f32[1024]{0:T(1024)} %param.33) | copy-start | bytes 12292
  20.0 8.2 %all-to-all-start.1 = ((bf16[4,16,1024]{2,1,0:T(8,128)(2,1)}), bf16[4,16,1024]{2,1,0:T(8,128)(2,1)S(1)}, u32[]{:S(2)}, u32[]{:S(2)}) async-start(bf16[4,16,1024]{2,1,0:T(8,128)(2,1)} %get-tuple-element.46), calls=%async_computation.1 | async-start | bytes 262144 | tf_op jit(solution)/shard_map/all_to_all | solution.py:214
  23.9 21.0 %collective-permute-start = (bf16[1536,256]{1,0:T(8,128)(2,1)}, bf16[1536,256]{1,0:T(8,128)(2,1)S(1)}, u32[]{:S(2)}, u32[]{:S(2)}) collective-permute-start(bf16[1536,256]{1,0:T(8,128)(2,1)} %bitcast_dynamic-update-slice_fusion), channel_id=1, source_target_pairs={{0,1},{1,0},{2,3},{3,2},{4,5},{5,4},{6,7},{7,6},{8,9},{9,8},{10,11... | collective-permute-start | bytes 2359304 | tf_op jit(solution)/shard_map/ppermute | solution.py:286
  30.8 29.4 %all-to-all-start.2 = ((bf16[128,8,128]{2,1,0:T(8,128)(2,1)}), bf16[128,8,128]{2,1,0:T(8,128)(2,1)S(1)}, u32[]{:S(2)}, u32[]{:S(2)}) async-start(bf16[128,8,128]{2,1,0:T(8,128)(2,1)} %bitcast.14), calls=%async_computation.2 | async-start | bytes 524288 | tf_op jit(solution)/shard_map/all_to_all | solution.py:214
  82.7 23.2 %copy-start.4 = (f32[16,256]{1,0:T(8,128)S(1)}, f32[16,256]{1,0:T(8,128)}, u32[]{:S(2)}) copy-start(f32[16,256]{1,0:T(8,128)} %dynamic-slice_convert_fusion) | copy-start | bytes 49156
  82.7 23.2 %copy-start.7 = (f32[16,1]{0,1:T(1,128)S(1)}, f32[16,1]{0,1:T(1,128)}, u32[]{:S(2)}) copy-start(f32[16,1]{0,1:T(1,128)} %get-tuple-element.61) | copy-start | bytes 196
  82.7 23.2 %copy-start.8 = (f32[16,1]{0,1:T(1,128)S(1)}, f32[16,1]{0,1:T(1,128)}, u32[]{:S(2)}) copy-start(f32[16,1]{0,1:T(1,128)} %get-tuple-element.60) | copy-start | bytes 196
  82.7 23.2 %copy-start.10 = (f32[16,1]{0,1:T(1,128)S(1)}, f32[16,1]{0,1:T(1,128)}, u32[]{:S(2)}) copy-start(f32[16,1]{0,1:T(1,128)} %divide_bitcast_fusion) | copy-start | bytes 196
